TPU v7x, 256 devices: a whole 4x4x8 slice. The times are simulated.
256 devices in a mesh: sp: 32 (over z, x), fs: 4 (over y), tp: 2 (over core).
Axes of the slice: x: 4, y: 4, z: 8, core: 2. Of those that a mesh axis runs over, the one named last changes fastest.
Arguments:
- tokens: bfloat16 [4, 4096, 2048], P('fs', 'sp', 'tp'), may hold values from -6 to 6
- norm_gain: float32 [2048], replicated, may hold values from 0.1 to 1.9
- retain_query: bfloat16 [2048, 512], P('fs', 'tp'), may hold values from -0.125 to 0.125
- retain_key: bfloat16 [2048, 512], P('fs', 'tp'), may hold values from -0.125 to 0.125
- retain_value: bfloat16 [2048, 1024], P('fs', 'tp'), may hold values from -0.125 to 0.125
- retain_gate: bfloat16 [2048, 1024], P('fs', 'tp'), may hold values from -0.125 to 0.125
- differ_query: bfloat16 [2048, 1024], P('fs', 'tp'), may hold values from -0.125 to 0.125
- differ_key: bfloat16 [2048, 1024], P('fs', 'tp'), may hold values from -0.125 to 0.125
- differ_value: bfloat16 [2048, 1024], P('fs', 'tp'), may hold values from -0.125 to 0.125
- log_decay: float32 [4, 4096, 4], P('fs', 'sp', 'tp'), may hold values from -0.8 to 0
- lambdas: float32 [8], P('tp'), may hold values from 0.3 to 0.8
- query_gain: float32 [8, 2, 64], P('tp'), may hold values from 1 to 9
- key_gain: float32 [8, 2, 64], P('tp'), may hold values from 1 to 9
- retain_gain: float32 [1024], P('tp'), may hold values from 0.1 to 1.9
- differ_gain: float32 [1024], P('tp'), may hold values from 0.1 to 1.9
- retain_out: bfloat16 [1024, 2048], P('tp', 'fs'), may hold values from -0.1875 to 0.1875
- differ_out: bfloat16 [1024, 2048], P('tp', 'fs'), may hold values from -0.1875 to 0.1875
Outputs:
- mixed: bfloat16 [4, 4096, 2048], P('fs', ('sp', 'tp'))
All inputs are finite; a program needn't handle non-finite values.
Results may differ from a plain program's by a relative error of at most 0.014.
The roundings to bfloat16 on the way count: a program that leaves them out, or rounds other values in their place, can miss the bound.
Values may be sent and summed in bfloat16 or wider, within the bound.
A program may use at most 128 MiB of HBM per device.

v0:
```python
import jax
import jax.numpy as jnp
from jax import lax
from jax.sharding import PartitionSpec as P

RET_DK = 128
RET_DV = 256
DIFF_HD = 64
DIFF_DV = 128
GRID_W = 64


EPSILON = 1e-06
ROPE_BASE = 10000.0


def laid_out(pieces, dim):
    pieces = jnp.moveaxis(pieces, 0, dim)
    shape = pieces.shape
    return pieces.reshape(*shape[:dim], shape[dim] * shape[dim + 1], *shape[dim + 2 :])


def sent_to_all(x, axis):
    copies = jnp.broadcast_to(x, (lax.axis_size(axis), *x.shape))
    return lax.all_to_all(copies, axis, split_axis=0, concat_axis=0, tiled=True)


def collect(x, axis, dim):
    return laid_out(sent_to_all(x, axis), dim)


def sent_together(arrays, axis, dim, along):
    both = jnp.concatenate(arrays, axis=along)
    whole, at, gathered = (lax.all_gather(both, axis, axis=dim, tiled=True), 0, [])
    for a in arrays:
        gathered.append(lax.slice_in_dim(whole, at, at + a.shape[along], axis=along))
        at += a.shape[along]
    return tuple(gathered)


def cut_along(x, dim, length):
    shape = x.shape
    pieces = x.reshape(*shape[:dim], length, shape[dim] // length, *shape[dim + 1 :])
    return jnp.moveaxis(pieces, dim, 0)


def sum_at_owner(x, axis, dim):
    length = lax.axis_size(axis)
    pieces = lax.all_to_all(cut_along(x, dim, length), axis, 0, 0, tiled=True)
    return jnp.sum(pieces.astype(jnp.float32), axis=0)


def rotate_half(vector, positions):
    length = vector.shape[-1]
    inverse = jnp.power(ROPE_BASE, -jnp.arange(0, length, 2, dtype=jnp.float32) / length)
    angles = positions.astype(jnp.float32)[:, None] * inverse[None, :]
    target_shape = (positions.shape[0],) + (1,) * (vector.ndim - 2) + (length // 2,)
    cosine = jnp.cos(angles).reshape(target_shape)
    sine_part = jnp.sin(angles).reshape(target_shape)
    leading = vector[..., : length // 2]
    trailing = vector[..., length // 2 :]
    return jnp.concatenate(
        [leading * cosine - trailing * sine_part, trailing * cosine + leading * sine_part], axis=-1
    )


def rotary_grid(vector, positions):
    middle = vector.shape[-1] // 2
    return jnp.concatenate(
        [
            rotate_half(vector[..., :middle], positions // GRID_W),
            rotate_half(vector[..., middle:], positions % GRID_W),
        ],
        axis=-1,
    )


def rms_scale(vector, gain_row):
    return (
        vector * lax.rsqrt(jnp.mean(vector * vector, axis=-1, keepdims=True) + EPSILON) * gain_row
    )


def retention_branch(queries, key_rows, value_rows, gate_rows, decay_rows, retain_gain):
    row_count = queries.shape[0]
    head_count = decay_rows.shape[1]
    levels = jnp.cumsum(decay_rows, axis=0)
    final_level = levels[-1]
    key_wide = key_rows.astype(jnp.float32)
    value_wide = value_rows.astype(jnp.float32)
    forward_own = jnp.einsum(
        "shd,shv->hdv", key_wide * jnp.exp(final_level - levels)[..., None], value_wide
    )
    backward_own = jnp.einsum("shd,shv->hdv", key_wide * jnp.exp(levels)[..., None], value_wide)
    level_table = collect(final_level[None], "sp", 0)
    inclusive = jnp.cumsum(level_table, axis=0)
    exclusive = inclusive - level_table
    own_index = lax.axis_index("sp")
    own_before = lax.dynamic_index_in_dim(exclusive, own_index, 0, keepdims=False)
    own_through = lax.dynamic_index_in_dim(inclusive, own_index, 0, keepdims=False)
    forward_piece, backward_piece = tuple(
        (
            part.astype(jnp.float32)
            for part in sent_together(
                (forward_own[None].astype(jnp.bfloat16), backward_own[None].astype(jnp.bfloat16)),
                "sp",
                0,
                1,
            )
        )
    )
    piece_rows = forward_piece.shape[0]
    indices = jnp.arange(piece_rows, dtype=jnp.int32)
    forward_gap = jnp.where(
        (indices < own_index)[:, None], own_before[None, :] - inclusive, -jnp.inf
    )
    backward_gap = jnp.where(
        (indices > own_index)[:, None], exclusive - own_through[None, :], -jnp.inf
    )
    forward_sum = jnp.zeros_like(forward_own) + jnp.einsum(
        "jh,jhdv->hdv", jnp.exp(forward_gap), forward_piece
    )
    backward_sum = jnp.zeros_like(backward_own) + jnp.einsum(
        "jh,jhdv->hdv", jnp.exp(backward_gap), backward_piece
    )
    query_wide = queries.astype(jnp.float32)
    carried = jnp.einsum("thd,hdv->thv", query_wide * jnp.exp(levels)[..., None], forward_sum)
    carried = carried + jnp.einsum(
        "thd,hdv->thv", query_wide * jnp.exp(final_level - levels)[..., None], backward_sum
    )
    scores = jnp.einsum("thd,shd->hts", queries, key_rows, preferred_element_type=jnp.float32)
    nearness = jnp.exp(-jnp.abs(levels.T[:, :, None] - levels.T[:, None, :]))
    weights = (scores * nearness).astype(jnp.bfloat16)
    inside = jnp.einsum("hts,shv->thv", weights, value_rows, preferred_element_type=jnp.float32)
    scaled = rms_scale(inside + carried, retain_gain.reshape(head_count, -1))
    return (jax.nn.silu(gate_rows.astype(jnp.float32)) * scaled.reshape(row_count, -1)).astype(
        jnp.bfloat16
    )


def contrast_branch(queries, key_rows, value_rows, lambdas, differ_gain):
    row_count = queries.shape[0]
    head_count = lambdas.shape[0]
    query_heads = queries.reshape(row_count, head_count, 2, DIFF_HD)
    score_scale = DIFF_HD ** (-0.5)

    def absorb_block(running, block_pair):
        maxima, totals, numerators = running
        key_block, value_block = block_pair
        scores = (
            jnp.einsum(
                "qhmd,khmd->mhqk", query_heads, key_block, preferred_element_type=jnp.float32
            )
            * score_scale
        )
        new_maxima = jnp.maximum(maxima, jnp.max(scores, axis=-1))
        exponent = jnp.exp(scores - new_maxima[..., None])
        shrink = jnp.exp(maxima - new_maxima)
        totals = totals * shrink + jnp.sum(exponent, axis=-1)
        numerators = numerators * shrink[..., None] + jnp.einsum(
            "mhqk,khv->mhqv",
            exponent.astype(jnp.bfloat16),
            value_block,
            preferred_element_type=jnp.float32,
        )
        return ((new_maxima, totals, numerators), None)

    initial = (
        jnp.full((2, head_count, row_count), -jnp.inf, jnp.float32),
        jnp.zeros((2, head_count, row_count), jnp.float32),
        jnp.zeros((2, head_count, row_count, DIFF_DV), jnp.float32),
    )
    running = initial
    key_piece, value_piece = sent_together((key_rows, value_rows), "sp", 0, 1)
    piece_rows = key_piece.shape[0]
    step_rows = max(
        (divisor for divisor in range(1, min(piece_rows, 1024) + 1) if piece_rows % divisor == 0)
    )
    key_blocks = key_piece.reshape(piece_rows // step_rows, step_rows, head_count, 2, DIFF_HD)
    value_blocks = value_piece.reshape(piece_rows // step_rows, step_rows, head_count, DIFF_DV)
    running, ignored = lax.scan(absorb_block, running, (key_blocks, value_blocks))
    maxima, totals, numerators = running
    ratios = numerators / totals[..., None]
    contrast_mix = ratios[0] - lambdas[:, None, None] * ratios[1]
    scaled = rms_scale(contrast_mix, differ_gain.reshape(head_count, 1, DIFF_DV))
    return jnp.transpose(scaled, (1, 0, 2)).reshape(row_count, -1).astype(jnp.bfloat16)


def body(
    tokens,
    norm_gain,
    retain_query,
    retain_key,
    retain_value,
    retain_gate,
    differ_query,
    differ_key,
    differ_value,
    log_decay,
    lambdas,
    query_gain,
    key_gain,
    retain_gain,
    differ_gain,
    retain_out,
    differ_out,
):
    gathered = collect(tokens[0], "tp", 1)
    row_count = gathered.shape[0]
    normed = rms_scale(gathered.astype(jnp.float32), norm_gain).astype(jnp.bfloat16)
    matrices = (
        retain_query,
        retain_key,
        retain_value,
        retain_gate,
        differ_query,
        differ_key,
        differ_value,
    )
    spread = lax.all_to_all(normed, "fs", split_axis=1, concat_axis=0, tiled=True)
    joined = jnp.concatenate(matrices, axis=1)
    summed = lax.psum_scatter(
        jnp.dot(spread, joined, preferred_element_type=jnp.float32),
        "fs",
        scatter_dimension=0,
        tiled=True,
    )
    column_edges = [0]
    for matrix in matrices:
        column_edges.append(column_edges[-1] + matrix.shape[1])
    projected = tuple(
        (
            summed[:, column_edges[matrix_index] : column_edges[matrix_index + 1]]
            for matrix_index in range(len(matrices))
        )
    )
    query_part, key_part, value_part, gate_part, cquery_part, ckey_part, cvalue_part = projected
    positions = lax.axis_index("sp") * row_count + jnp.arange(row_count, dtype=jnp.int32)
    decay_rows = log_decay[0]
    retain_heads = decay_rows.shape[1]
    differ_heads = lambdas.shape[0]
    retention_query = rotary_grid(
        query_part.reshape(row_count, retain_heads, RET_DK), positions
    ).astype(jnp.bfloat16)
    retention_keys = (
        rotary_grid(key_part.reshape(row_count, retain_heads, RET_DK), positions) * RET_DK ** (-0.5)
    ).astype(jnp.bfloat16)
    retention_values = value_part.astype(jnp.bfloat16).reshape(row_count, retain_heads, RET_DV)
    retention_gate = gate_part.astype(jnp.bfloat16)
    contrast_query = (
        rotary_grid(
            rms_scale(cquery_part.reshape(row_count, differ_heads, 2, DIFF_HD), query_gain),
            positions,
        )
        .astype(jnp.bfloat16)
        .reshape(row_count, -1)
    )
    contrast_keys = (
        rotary_grid(
            rms_scale(ckey_part.reshape(row_count, differ_heads, 2, DIFF_HD), key_gain), positions
        )
        .astype(jnp.bfloat16)
        .reshape(row_count, -1)
    )
    contrast_values = cvalue_part.astype(jnp.bfloat16)
    contrast_features = contrast_branch(
        contrast_query, contrast_keys, contrast_values, lambdas, differ_gain
    )
    retention_features = retention_branch(
        retention_query, retention_keys, retention_values, retention_gate, decay_rows, retain_gain
    )
    retain_columns, differ_columns = sent_together((retain_out, differ_out), "fs", 1, 0)
    summed_out = sum_at_owner(
        (
            jnp.dot(retention_features, retain_columns, preferred_element_type=jnp.float32)
            + jnp.dot(contrast_features, differ_columns, preferred_element_type=jnp.float32)
        ).astype(jnp.bfloat16),
        "tp",
        0,
    )
    return summed_out.astype(jnp.bfloat16)[None]


def solution(mesh):
    in_specs = (
        P("fs", "sp", "tp"),
        P(),
        P("fs", "tp"),
        P("fs", "tp"),
        P("fs", "tp"),
        P("fs", "tp"),
        P("fs", "tp"),
        P("fs", "tp"),
        P("fs", "tp"),
        P("fs", "sp", "tp"),
        P("tp"),
        P("tp", None, None),
        P("tp", None, None),
        P("tp"),
        P("tp"),
        P("tp", "fs"),
        P("tp", "fs"),
    )
    out_specs = P("fs", ("sp", "tp"), None)
    return jax.shard_map(body, mesh=mesh, in_specs=in_specs, out_specs=out_specs, check_vma=False)
```

profile of v0, /device:TPU:1, one launch (start us, length us, event | category | flops | bytes accessed | tf_op | source)
XLA Modules:
  0.0 369.1 jit_solution(4897799096379900294)
XLA Ops:
  6.5 1.1 copy.86
  7.7 7.1 %all_to_all.31 = bf16[2,128,1024]{1,2,0:T(8,128)(2,1)S(1)} all-to-all(bf16[2,128,1024]{1,2,0:T(8,128)(2,1)S(1)} %broadcast_in_dim.26), channel_id=1, replica_groups=mesh['sp'=32,'fs'=4,'tp'=2] {'tp'}, dimensions={0} | all-to-all | bytes 1048576 | tf_op jit(solution)/shard_map/all_to_all | solution.py:25
  15.1 0.7 mul.257
  15.9 1.1 multiply_convert_fusion
  17.0 4.1 %all-to-all-start.1 = ((bf16[128,4,512]{0,2,1:T(8,128)(2,1)}), bf16[128,4,512]{0,2,1:T(8,128)(2,1)}, u32[]{:S(2)}, u32[]{:S(2)}) async-start(bf16[128,4,512]{0,2,1:T(8,128)(2,1)} %multiply_convert_fusion), calls=%async_computation.1 | async-start | bytes 1048576 | tf_op jit(solution)/shard_map/all_to_all | solution.py:220
  21.3 1.0 constant_dynamic-update-slice_fusion.5
  22.3 1.1 constant_dynamic-update-slice_fusion.4
  23.4 1.1 constant_dynamic-update-slice_fusion.3
  24.5 1.1 constant_dynamic-update-slice_fusion.2
  25.6 1.1 constant_dynamic-update-slice_fusion.1
  26.7 1.1 constant_dynamic-update-slice_fusion
  27.8 2.6 all-to-all-done.1
  30.4 2.0 copy.87
  32.5 5.5 %fusion.64 = f32[512,3072]{1,0:T(8,128)} fusion(bf16[512,512]{1,0:T(8,128)(2,1)} %bitcast.120, bf16[512,3072]{1,0:T(8,128)(2,1)S(1)} %constant_dynamic-update-slice_fusion), kind=kOutput, calls=%fused_computation.153 | convolution fusion | flops 1610612736 | bytes 9961472 | tf_op jit(solution)/shard_map/dot_general | solution.py:223
  38.3 66.3 %reduce-scatter.2.cloned.1.call-done = f32[128,3072]{1,0:T(8,128)} async-done(((f32[512,3072]{1,0:T(8,128)}), f32[128,3072]{1,0:T(8,128)}) %reduce-scatter.2.cloned.1.call-update) | async-done | bytes 1572880 | tf_op jit(solution)/shard_map/reduce_scatter | solution.py:222
  104.5 1.2 fusion.59
  106.4 0.9 copy-done.1
  107.3 0.7 pad_maximum_fusion.2
  108.6 0.5 multiply_cosine_fusion.1
  109.3 0.5 fusion.62
  109.8 0.5 fusion.63
  110.9 0.3 fusion.24
  111.2 0.7 pad_maximum_fusion.1
  112.0 0.6 broadcast_in_dim.30
  112.6 9.5 %all-to-all-start.2 = ((f32[32,1,2]{2,1,0:T(1,128)}), f32[32,1,2]{2,1,0:T(1,128)S(1)}, u32[]{:S(2)}, u32[]{:S(2)}) async-start(f32[32,1,2]{2,1,0:T(1,128)} %broadcast_in_dim.30), calls=%async_computation.3 | async-start | bytes 32768 | tf_op jit(solution)/shard_map/all_to_all | solution.py:25
  122.4 1.1 pad_maximum_fusion
  123.7 0.6 mul.563
  124.3 6.3 %all-to-all-done.2 = f32[32,1,2]{2,1,0:T(1,128)S(1)} async-done(((f32[32,1,2]{2,1,0:T(1,128)}), f32[32,1,2]{2,1,0:T(1,128)S(1)}, u32[]{:S(2)}, u32[]{:S(2)}) %all-to-all-start.2) | async-done | bytes 288 | tf_op jit(solution)/shard_map/all_to_all | solution.py:25
  130.9 0.7 exponential_bitcast_fusion
  131.6 0.7 exponential_bitcast_fusion.1
  132.8 0.4 fusion.26
  133.2 72.0 %all-gather.8.cloned.1.call-done = bf16[4096,1024]{1,0:T(8,128)(2,1)} async-done(((bf16[128,1024]{1,0:T(8,128)(2,1)}), bf16[4096,1024]{1,0:T(8,128)(2,1)}) %all-gather.8.cloned.1.call-update) | async-done | bytes 8388624 | tf_op jit(solution)/shard_map/all_gather | solution.py:34
  205.2 5.8 %fusion.58 = (bf16[4096,512]{1,0:T(8,128)(2,1)}, bf16[4096,512]{1,0:T(8,128)(2,1)}) fusion(bf16[4096,1024]{1,0:T(8,128)(2,1)} %all-gather.8.cloned.1.call-done), kind=kLoop, calls=%fused_computation.147 | loop fusion | bytes 16777216 | tf_op jit(solution)/shard_map/slice | solution.py:36
  211.0 16.0 %reshape.403 = bf16[4,1024,4,2,64]{4,3,2,1,0:T(2,128)(2,1)} reshape(bf16[4096,512]{1,0:T(8,128)(2,1)} %get-tuple-element.115) | data formatting | bytes 8388608 | tf_op jit(solution)/shard_map/reshape | solution.py:179
  227.0 20.2 %copy.114 = bf16[4,1024,4,2,64]{1,4,2,3,0:T(8,128)(2,1)} copy(bf16[4,1024,4,2,64]{4,3,2,1,0:T(2,128)(2,1)} %reshape.403) | data formatting | bytes 8388608
  247.2 6.9 %reshape.395 = bf16[4,1024,4,128]{3,2,1,0:T(4,128)(2,1)} reshape(bf16[4096,512]{1,0:T(8,128)(2,1)} %get-tuple-element.114) | data formatting | bytes 8388608 | tf_op jit(solution)/shard_map/reshape | solution.py:180
  254.1 51.5 %while.15 = (s32[]{:T(128)}, f32[2,4,128]{2,1,0:T(4,128)S(1)}, f32[2,4,128]{2,1,0:T(4,128)S(1)}, f32[2,4,128,128]{2,3,0,1:T(8,128)}, bf16[4,1024,4,2,64]{1,4,2,3...) while((s32[]{:T(128)}, f32[2,4,128]{2,1,0:T(4,128)S(1)}, ...), condition=%wide.region_10.11_spmd.clone, body=%wide.region_7.10_spmd.clone.sunk | while | flops 409342976 | bytes 20124268 | solution.py:181
  254.1 4.0 %bitcast_reduce_fusion.2 = (f32[2,4,128]{2,1,0:T(4,128)S(1)}, f32[2,4,1024,128]{3,2,1,0:T(8,128)}) fusion(bf16[128,4,2,64]{0,3,1,2:T(8,128)(2,1)S(1)} %get-tuple-element.252, bf16[4,1024,4,2,64]{1,4,2,3,0:T(8,128)(2,1)} %get-tuple-element.251, s32[]{:T(128)} %get-tuple-element.238), kind=kOutput, calls=%fused_computation.1.clone.1 | convolution fusion | flops 136313856 | bytes 5378560 | tf_op jit(solution)/shard_map/while/body/eval_jaxpr/qhmd,khmd->mhqk/dot_general | solution.py:151
  258.1 3.0 fusion.82
  261.2 1.6 constant_dynamic-slice_fusion.2
  262.8 1.5 copy.194
  264.3 2.5 fusion.84
  266.8 4.0 %bitcast_reduce_fusion.2 = (f32[2,4,128]{2,1,0:T(4,128)S(1)}, f32[2,4,1024,128]{3,2,1,0:T(8,128)}) fusion(bf16[128,4,2,64]{0,3,1,2:T(8,128)(2,1)S(1)} %get-tuple-element.252, bf16[4,1024,4,2,64]{1,4,2,3,0:T(8,128)(2,1)} %get-tuple-element.251, s32[]{:T(128)} %get-tuple-element.238), kind=kOutput, calls=%fused_computation.1.clone.1 | convolution fusion | flops 136313856 | bytes 5378560 | tf_op jit(solution)/shard_map/while/body/eval_jaxpr/qhmd,khmd->mhqk/dot_general | solution.py:151
  270.8 3.2 fusion.82
  274.0 1.6 constant_dynamic-slice_fusion.2
  275.6 1.5 copy.194
  277.1 2.7 fusion.84
  279.9 4.0 %bitcast_reduce_fusion.2 = (f32[2,4,128]{2,1,0:T(4,128)S(1)}, f32[2,4,1024,128]{3,2,1,0:T(8,128)}) fusion(bf16[128,4,2,64]{0,3,1,2:T(8,128)(2,1)S(1)} %get-tuple-element.252, bf16[4,1024,4,2,64]{1,4,2,3,0:T(8,128)(2,1)} %get-tuple-element.251, s32[]{:T(128)} %get-tuple-element.238), kind=kOutput, calls=%fused_computation.1.clone.1 | convolution fusion | flops 136313856 | bytes 5378560 | tf_op jit(solution)/shard_map/while/body/eval_jaxpr/qhmd,khmd->mhqk/dot_general | solution.py:151
  283.9 3.1 fusion.82
  287.0 1.6 constant_dynamic-slice_fusion.2
  288.6 1.5 copy.194
  290.1 2.7 fusion.84
  292.8 4.0 %bitcast_reduce_fusion.2 = (f32[2,4,128]{2,1,0:T(4,128)S(1)}, f32[2,4,1024,128]{3,2,1,0:T(8,128)}) fusion(bf16[128,4,2,64]{0,3,1,2:T(8,128)(2,1)S(1)} %get-tuple-element.252, bf16[4,1024,4,2,64]{1,4,2,3,0:T(8,128)(2,1)} %get-tuple-element.251, s32[]{:T(128)} %get-tuple-element.238), kind=kOutput, calls=%fused_computation.1.clone.1 | convolution fusion | flops 136313856 | bytes 5378560 | tf_op jit(solution)/shard_map/while/body/eval_jaxpr/qhmd,khmd->mhqk/dot_general | solution.py:151
  296.8 3.0 fusion.82
  299.8 1.6 constant_dynamic-slice_fusion.2
  301.4 1.5 copy.194
  302.9 2.7 fusion.84
  305.7 4.8 %multiply_reduce_fusion = (bf16[2,128,256]{2,1,0:T(8,128)(2,1)S(1)}, bf16[2,128,256]{2,1,0:T(8,128)(2,1)S(1)}) fusion(bf16[32,4,128,256]{3,2,1,0:T(8,128)(2,1)} %all-gather.4.cloned.1.call-done, f32[2,32]{0,1:T(8,128)} %get-tuple-element.108, f32[2,32]{0,1:T(8,128)} %exponential_bitcast_fusion.1), kind=kLoop, calls=%fused_computation.20 | loop fusion | flops 12451840 | bytes 8651264 | tf_op jit(solution)/shard_map/jh,jhdv->hdv/dot_general | solution.py:123
  310.8 0.3 multiply_reduce_fusion.6
  311.7 41.2 %all-gather.6.cloned.1.call-done = bf16[1024,2048]{1,0:T(8,128)(2,1)} async-done(((bf16[1024,512]{1,0:T(8,128)(2,1)}), bf16[1024,2048]{1,0:T(8,128)(2,1)}) %all-gather.6.cloned.1.call-update) | async-done | bytes 4194320 | tf_op jit(solution)/shard_map/all_gather | solution.py:34
  352.9 2.1 fusion.19
  355.1 2.1 fusion.17
  357.1 4.6 %all_to_all.32 = bf16[2,64,2048]{2,1,0:T(8,128)(2,1)S(1)} all-to-all(bf16[2,64,2048]{2,1,0:T(8,128)(2,1)S(1)} %bitcast.124), channel_id=1, replica_groups=mesh['sp'=32,'fs'=4,'tp'=2] {'tp'}, dimensions={0} | all-to-all | bytes 1048576 | tf_op jit(solution)/shard_map/all_to_all | solution.py:49
  361.8 0.8 reduce_sum.71
  (117 shorter events, 4.7 us)
Async XLA Ops:
  7.7 13.6 %copy-start.7 = (bf16[512,256]{1,0:T(8,128)(2,1)S(1)}, bf16[512,256]{1,0:T(8,128)(2,1)}, u32[]{:S(2)}) copy-start(bf16[512,256]{1,0:T(8,128)(2,1)} %param.21) | copy-start | bytes 786436
  17.0 13.4 %all-to-all-start.1 = ((bf16[128,4,512]{0,2,1:T(8,128)(2,1)}), bf16[128,4,512]{0,2,1:T(8,128)(2,1)}, u32[]{:S(2)}, u32[]{:S(2)}) async-start(bf16[128,4,512]{0,2,1:T(8,128)(2,1)} %multiply_convert_fusion), calls=%async_computation.1 | async-start | bytes 1048576 | tf_op jit(solution)/shard_map/all_to_all | solution.py:220
  21.2 83.4 %reduce-scatter.2.cloned.1.call-start = ((), (), s32[]{:S(2)}) async-start(), calls=%async_computation.5 | async-start | bytes 7864320 | tf_op jit(solution)/shard_map/reduce_scatter | solution.py:222
  38.0 67.9 %copy-start.11 = (f32[4,2,64]{2,1,0:T(2,128)S(1)}, f32[4,2,64]{2,1,0:T(2,128)}, u32[]{:S(2)}) copy-start(f32[4,2,64]{2,1,0:T(2,128)} %param.31) | copy-start | bytes 6148
  38.0 167.2 %all-gather.8.cloned.1.call-start = ((), (), s32[]{:S(2)}) async-start(), calls=%async_computation.8 | async-start | bytes 8650752 | tf_op jit(solution)/shard_map/all_gather | solution.py:34
  104.5 1.7 copy-start
  105.7 2.4 copy-start.16
  106.4 0.9 copy-start.1
  108.0 197.6 %all-gather.4.cloned.1.call-start = ((), (), s32[]{:S(2)}) async-start(), calls=%async_computation.6 | async-start | bytes 8650752 | tf_op jit(solution)/shard_map/all_gather | solution.py:34
  108.5 2.5 copy-start.8
  109.3 13.1 %copy-start.5 = (bf16[512,512]{1,0:T(8,128)(2,1)S(1)}, bf16[512,512]{1,0:T(8,128)(2,1)}, u32[]{:S(2)}) copy-start(bf16[512,512]{1,0:T(8,128)(2,1)} %param.35) | copy-start | bytes 1572868
  109.3 13.1 %copy-start.6 = (bf16[512,512]{1,0:T(8,128)(2,1)S(1)}, bf16[512,512]{1,0:T(8,128)(2,1)}, u32[]{:S(2)}) copy-start(bf16[512,512]{1,0:T(8,128)(2,1)} %param.34) | copy-start | bytes 1572868
  110.4 13.3 %copy-start.14 = (f32[512]{0:T(512)S(1)}, f32[512]{0:T(512)}, u32[]{:S(2)}) copy-start(f32[512]{0:T(512)} %param.32) | copy-start | bytes 6148
  110.4 22.0 %copy-start.12 = (f32[4,2,64]{2,1,0:T(2,128)S(1)}, f32[4,2,64]{2,1,0:T(2,128)}, u32[]{:S(2)}) copy-start(f32[4,2,64]{2,1,0:T(2,128)} %param.30) | copy-start | bytes 6148
  112.6 18.0 %all-to-all-start.2 = ((f32[32,1,2]{2,1,0:T(1,128)}), f32[32,1,2]{2,1,0:T(1,128)S(1)}, u32[]{:S(2)}, u32[]{:S(2)}) async-start(f32[32,1,2]{2,1,0:T(1,128)} %broadcast_in_dim.30), calls=%async_computation.3 | async-start | bytes 32768 | tf_op jit(solution)/shard_map/all_to_all | solution.py:25
  122.2 230.8 %all-gather.6.cloned.1.call-start = ((), (), s32[]{:S(2)}) async-start(), calls=%async_computation.7 | async-start | bytes 5242880 | tf_op jit(solution)/shard_map/all_gather | solution.py:34
  132.8 78.2 %copy-start.2 = (bf16[128,2,128]{2,0,1:T(8,128)(2,1)}, bf16[128,2,128]{2,0,1:T(8,128)(2,1)S(1)}, u32[]{:S(2)}) copy-start(bf16[128,2,128]{2,0,1:T(8,128)(2,1)S(1)} %pad_maximum_fusion.5) | copy-start | bytes 196612
  305.6 4.8 %copy-start.3 = (bf16[128,2,128]{2,0,1:T(8,128)(2,1)S(1)}, bf16[128,2,128]{2,0,1:T(8,128)(2,1)}, u32[]{:S(2)}) copy-start(bf16[128,2,128]{2,0,1:T(8,128)(2,1)} %copy-done.2) | copy-start | bytes 196612
  305.7 5.1 %copy-start.9 = (f32[128,2]{0,1:T(2,128)S(1)}, f32[128,2]{0,1:T(2,128)}, u32[]{:S(2)}) copy-start(f32[128,2]{0,1:T(2,128)} %copy-done.8) | copy-start | bytes 3076
  305.7 5.4 %copy-start.10 = (f32[2,256]{1,0:T(2,128)S(1)}, f32[2,256]{1,0:T(2,128)}, u32[]{:S(2)}) copy-start(f32[2,256]{1,0:T(2,128)} %mul.563) | copy-start | bytes 6148
  305.7 5.7 %copy-start.4 = (f32[2,4,128,128]{2,3,0,1:T(8,128)S(1)}, f32[2,4,128,128]{2,3,0,1:T(8,128)}, u32[]{:S(2)}) copy-start(f32[2,4,128,128]{2,3,0,1:T(8,128)} %get-tuple-element.43) | copy-start | bytes 1572868
  310.5 1.0 copy-start.15
  310.5 1.1 copy-start.13
Sparse Core Ops, SparseCore 0:
  38.1 66.3 reduce-scatter.1
  108.1 96.9 all-gather.7
  207.8 94.9 all-gather.3
  304.4 48.5 all-gather.5
where the time goes:
time: 371 us; the launch traced here: 369 us
  waiting for transfers between devices  188 us (51%)
  local copies, waits for them, and re-layouts  77.4 us (21%)
  matrix products  37.7 us (10%)
  other arithmetic  25.9 us (7%)
  starting transfers between devices  14 us (4%)
  between operations  13.8 us (4%)
  blocking collectives  11.7 us (3%)
    all_gather x3, waiting for transfers between devices, sent_together(): lax.all_gather(both, axis, axis=dim, tiled=True)  113 us
    reduce_scatter x1, waiting for transfers between devices, body(): lax.psum_scatter(jnp.dot(spread, joined, preferred_element_type=jnp.float...  66.3 us
    unnamed x42, local copies, waits for them, and re-layouts  26.6 us
    reshape x1, local copies, waits for them, and re-layouts, contrast_branch(): key_piece.reshape(piece_rows // step_rows, step_rows, head_count, 2, DIFF...  16 us
    dot_general x4, matrix products, absorb_block(): jnp.einsum('qhmd,khmd->mhqk', query_heads, key_block, preferred_element_t...  16 us
    dynamic_slice x8, local copies, waits for them, and re-layouts, contrast_branch(): lax.scan(absorb_block, running, (key_blocks, value_blocks))  12.4 us
    convert_element_type x4, other arithmetic, absorb_block(): exponent.astype(jnp.bfloat16)  12.3 us
    dot_general x4, matrix products, absorb_block(): jnp.einsum('mhqk,khv->mhqv', exponent.astype(jnp.bfloat16), value_block,...  10.6 us
  transfers between devices with their start and end apart: 6, of which 5 were waited for; matrix products, arithmetic and copies ran while one was open for 33% of the time, Pallas kernels for 0%

commit v1 on v0

v1 whole, which is shorter than its diff:
```python
import functools

import numpy as np
import jax
import jax.numpy as jnp
from jax import lax
from jax.experimental import pallas as pl
from jax.experimental.pallas import tpu as pltpu
from jax.sharding import PartitionSpec as P

F32 = jnp.float32
BF16 = jnp.bfloat16
MESH = pl.DeviceIdType.MESH
EPS = 1e-06
ROPE_BASE = 10000.0
NX, NY, NZ = 4, 4, 8
ROWS = 128
BLOCK = NX * ROWS
D = 2048
WIDTHS = (256, 256, 256, 128)

TOK = 0
PART = 4
WG = 8
WO1 = 24
WO2 = 28
DEC = 40
KV = 43
ST = 59
DF = 75
GT = 78
RM = 81
OUT = 84
COPIES = 88
LOCALS = 16


def rope_tables():
    lane = np.arange(128)
    value = np.arange(64, dtype=np.float64)[:, None]
    tables = []
    for group in (32, 64):
        inverse = ROPE_BASE ** (-2.0 * ((lane % group) % (group // 2)) / group)
        angle = value * inverse[None, :]
        sign = np.where((lane % group) < group // 2, -1.0, 1.0)[None, :]
        tables += [np.cos(angle), np.sin(angle) * sign]
    return np.stack(tables).astype(np.float32)


def kernel(
    tok_in, w_rq, w_rk, w_rv, w_rg, w_dq, w_dk, w_dv, w_ro, w_do, dec_in, par, gain_in, tab,
    out,
    tok, xn, wg0, wg1, wg2, wg3, wo, dec, kb, vb, st, dz, cosd, sind, cosr, sinr, proj, qbd,
    m_run, l_run, acc, rq, rk, rv, grow, gcol, mix, gate, feat, df, gt, rm, fall, part, pin,
    ssem, rsem, lsem,
):
    sp = lax.axis_index("sp")
    z, x = sp // NX, sp % NX
    y = lax.axis_index("fs")
    c = lax.axis_index("tp")
    other = 1 - c

    def along_x(i):
        return {"sp": z * NX + i}

    def along_y(i):
        return {"fs": i}

    def along_z(i):
        return {"sp": i * NX + x}

    partner = {"tp": other}
    xs = [x, (x + 1) % NX, (x + 2) % NX, (x + 3) % NX]
    ys = [y, (y + 1) % NY, (y + 2) % NY, (y + 3) % NY]
    zr, zl = (z + 1) % NZ, (z + NZ - 1) % NZ

    def remote(i, src, dst, device):
        return pltpu.make_async_remote_copy(
            src_ref=src, dst_ref=dst, send_sem=ssem.at[i], recv_sem=rsem.at[i],
            device_id=device, device_id_type=MESH,
        )

    sent = []

    def send(i, src, dst, device):
        copy = remote(i, src, dst, device)
        copy.start()
        sent.append(copy)

    def arrived(i, ref):
        remote(i, ref, ref, partner).wait_recv()

    class Ring4:
        def __init__(self, base, at, device, full, half):
            self.base, self.at, self.device, self.full, self.half = base, at, device, full, half

        def own(self):
            block = self.full(self.at[0])
            send(self.base, block, block, self.device(self.at[1]))
            send(self.base + 1, block, block, self.device(self.at[3]))

        def forward(self):
            arrived(self.base, self.full(self.at[3]))
            a = self.half(self.at[3], 0)
            send(self.base + 2, a, a, self.device(self.at[1]))
            arrived(self.base + 1, self.full(self.at[1]))
            b = self.half(self.at[1], 1)
            send(self.base + 3, b, b, self.device(self.at[3]))

        def far(self):
            arrived(self.base + 2, self.half(self.at[2], 0))
            arrived(self.base + 3, self.half(self.at[2], 1))

    wgs = (wg0, wg1, wg2, wg3)
    token_ring = Ring4(
        TOK, xs, along_x,
        lambda i: tok.at[i, c],
        lambda i, h: tok.at[i, c, pl.ds(h * 64, 64)],
    )

    def weight_ring(g):
        ref = wgs[g]
        return Ring4(
            WG + 4 * g, ys, along_y,
            lambda i: ref.at[pl.ds(pl.multiple_of(i * 512, 512), 512)],
            lambda i, h: ref.at[pl.ds(pl.multiple_of(i * 512 + h * 256, 256), 256)],
        )

    rings = [weight_ring(g) for g in range(4)]
    out_ring1 = Ring4(
        WO1, ys, along_y,
        lambda i: wo.at[i, x],
        lambda i, h: wo.at[i, x, pl.ds(h * 128, 128)],
    )

    def out_ring2(k):
        yy = ys[k]
        return Ring4(
            WO2 + 4 * (k - 1), xs, along_x,
            lambda i: wo.at[yy, i],
            lambda i, h: wo.at[yy, i, pl.ds(h * 128, 128)],
        )

    rings2 = {k: out_ring2(k) for k in (1, 2, 3)}

    def local(i, src, dst):
        copy = pltpu.make_async_copy(src, dst, lsem.at[i])
        copy.start()
        return copy

    col = pl.ds(pl.multiple_of(x * 128, 128), 128)
    col2 = pl.ds(pl.multiple_of((x // 2) * 128, 128), 128)
    own_rows = pl.ds(pl.multiple_of(y * 512, 512), 512)
    lo, hi = pl.ds(0, 128), pl.ds(128, 128)
    load_tok = local(0, tok_in.at[0], tok.at[x, c])
    load_g = [
        [local(1, w_dk.at[:, col], wg0.at[own_rows, lo]), local(2, w_dv.at[:, col], wg0.at[own_rows, hi])],
        [local(3, w_dq.at[:, col], wg1.at[own_rows, lo]), local(4, w_rq.at[:, col2], wg1.at[own_rows, hi])],
        [local(5, w_rk.at[:, col2], wg2.at[own_rows, lo]), local(6, w_rv.at[:, col], wg2.at[own_rows, hi])],
        [local(7, w_rg.at[:, col], wg3.at[own_rows])],
    ]
    load_o = []
    for i in range(NX):
        load_o.append(local(8 + 2 * i, w_ro.at[pl.ds(i * 128, 128)], wo.at[y, i, lo]))
        load_o.append(local(9 + 2 * i, w_do.at[pl.ds(i * 128, 128)], wo.at[y, i, hi]))

    barrier = pltpu.get_barrier_semaphore()
    peers = [along_x(xs[1]), along_x(xs[2]), along_x(xs[3]), along_y(ys[1]), along_y(ys[3]),
             along_z(zr), along_z(zl), partner]
    for peer in peers:
        pl.semaphore_signal(barrier, inc=1, device_id=peer, device_id_type=MESH)
    pl.semaphore_wait(barrier, len(peers))

    load_tok.wait()
    token_ring.own()
    send(PART, tok.at[x, c], tok.at[x, c], partner)
    for copy in load_g[0]:
        copy.wait()
    rings[0].own()
    for d in (1, 2, 3):
        send(DEC + d - 1, dec_in, dec.at[x], along_x(xs[d]))
    dec[x] = dec_in[...]
    for group in load_g[1:]:
        for copy in group:
            copy.wait()
    for copy in load_o:
        copy.wait()

    lane = lax.broadcasted_iota(jnp.int32, (128, 128), 1)
    sub = lax.broadcasted_iota(jnp.int32, (128, 128), 0)

    lane64 = lax.broadcasted_iota(jnp.int32, (64, 128), 1)
    zrow = pl.ds(pl.multiple_of(z * 8, 8), 8)
    for k, ref in enumerate((cosd, sind, cosr, sinr)):
        by_row = tab[k, zrow, :]
        by_col = tab[k]
        is_row = (lane64 % 64) < 32 if k < 2 else lane64 < 64
        for b in range(8):
            ref[b * 64 : b * 64 + 64, :] = jnp.where(is_row, by_row[b : b + 1, :], by_col)

    def rope(u, cos, sin, group):
        half = group // 2
        up = pltpu.roll(u, 128 - half, 1)
        down = pltpu.roll(u, half, 1)
        return u * cos + jnp.where((lane % group) < half, up, down) * sin

    def map_norm(u, gain):
        square = u * u
        first = jnp.sum(jnp.where(lane < 64, square, 0.0), axis=-1, keepdims=True)
        second = jnp.sum(jnp.where(lane < 64, 0.0, square), axis=-1, keepdims=True)
        scale = jnp.where(
            lane < 64, lax.rsqrt(first / 64 + EPS), lax.rsqrt(second / 64 + EPS)
        )
        return u * scale * gain

    def normalize(i):
        def rows(j, carry):
            r = pl.ds(pl.multiple_of(j * 16, 16), 16)
            w = pl.ds(pl.multiple_of(i * 128 + j * 16, 16), 16)
            a = tok[i, 0, r, :].astype(F32)
            b = tok[i, 1, r, :].astype(F32)
            total = jnp.sum(a * a, axis=-1, keepdims=True) + jnp.sum(b * b, axis=-1, keepdims=True)
            scale = lax.rsqrt(total / D + EPS)
            xn[w, 0:1024] = (a * scale * gain_in[:, 0:1024]).astype(BF16)
            xn[w, 1024:2048] = (b * scale * gain_in[:, 1024:2048]).astype(BF16)
            return carry

        lax.fori_loop(0, 8, rows, 0)

    def project(g):
        ref = wgs[g]
        width = WIDTHS[g]

        def rows(j, carry):
            r = pl.ds(pl.multiple_of(j * 256, 256), 256)
            proj[r, 0:width] = jnp.dot(xn[r, :], ref[...], preferred_element_type=F32)
            return carry

        lax.fori_loop(0, 2, rows, 0)

    rings[0].forward()
    rings[1].own()
    out_ring1.own()

    token_ring.forward()
    send(PART + 1, tok.at[xs[3], c], tok.at[xs[3], c], partner)
    send(PART + 2, tok.at[xs[1], c], tok.at[xs[1], c], partner)
    arrived(PART, tok.at[x, other])
    normalize(xs[0])
    arrived(PART + 1, tok.at[xs[3], other])
    normalize(xs[3])
    arrived(PART + 2, tok.at[xs[1], other])
    normalize(xs[1])
    token_ring.far()
    send(PART + 3, tok.at[xs[2], c], tok.at[xs[2], c], partner)
    arrived(PART + 3, tok.at[xs[2], other])
    normalize(xs[2])

    rings[0].far()
    project(0)
    kgain = par[1:2, :]
    for i in range(NX):
        r = slice(i * 128, i * 128 + 128)
        u = map_norm(proj[r, 0:128], kgain)
        kb[z, r, :] = rope(u, cosd[r, :], sind[r, :], 32).astype(BF16)
        vb[z, :, r] = proj[r, 128:256].T.astype(BF16)

    zs = [(z + NZ + d) % NZ for d in range(-4, 5)]

    def at_z(d):
        return zs[d + 4]

    def kv_send(step, way, piece):
        origin = at_z(-step if way == 0 else step)
        ref = (kb, vb)[piece].at[origin]
        send(KV + 4 * step + 2 * way + piece, ref, ref, along_z(zr if way == 0 else zl))

    def kv_arrived(step, way, piece):
        origin = at_z(-(step + 1) if way == 0 else step + 1)
        arrived(KV + 4 * step + 2 * way + piece, (kb, vb)[piece].at[origin])

    for piece in (0, 1):
        for way in (0, 1):
            kv_send(0, way, piece)

    for d in (1, 2, 3):
        arrived(DEC + d - 1, dec.at[xs[4 - d]])
    lane8 = lax.broadcasted_iota(jnp.int32, (8, 128), 1)
    offset = jnp.zeros((1, 1), F32)
    head = x // 2
    for b in range(NX):
        level = dec[b]
        for k in (1, 2, 4, 8, 16, 32, 64):
            level = level + jnp.where(lane8 >= k, pltpu.roll(level, k, 1), 0.0)
        row = jnp.where(head == 0, level[0:1, :], level[1:2, :]) + offset
        offset = row[:, 127:128]
        grow[:, b * 128 : b * 128 + 128] = row
        gcol[b * 128 : b * 128 + 128, :] = jnp.broadcast_to(row, (128, 128)).T
    dz[z] = jnp.broadcast_to(offset, (8, 128))

    rings[1].forward()
    rings[2].own()
    rings[1].far()
    project(1)
    qgain = par[0:1, :]
    for i in range(NX):
        r = slice(i * 128, i * 128 + 128)
        u = map_norm(proj[r, 0:128], qgain)
        u = rope(u, cosd[r, :], sind[r, :], 32).astype(BF16).astype(F32) * 0.125
        u = u.T
        s = slice((i % 2) * 128, (i % 2) * 128 + 128)
        qbd[i // 2, :, s] = jnp.where(sub < 64, u, 0.0).astype(BF16)
        qbd[2 + i // 2, :, s] = jnp.where(sub < 64, 0.0, u).astype(BF16)
        rq[r, :] = rope(proj[r, 128:256], cosr[r, :], sinr[r, :], 64).astype(BF16)

    m_run[...] = jnp.full((4, 1, 256), -jnp.inf, F32)
    l_run[...] = jnp.zeros((4, 1, 256), F32)
    acc[...] = jnp.zeros((4, 128, 256), F32)

    def attend(origin):
        def tile(q, carry):
            s = jnp.dot(kb[origin], qbd[q], preferred_element_type=F32)
            before = m_run[q]
            now = jnp.maximum(before, jnp.max(s, axis=0, keepdims=True))
            shrink = jnp.exp(before - now)
            e = jnp.exp(s - now)
            m_run[q] = now
            l_run[q] = l_run[q] * shrink + jnp.sum(e, axis=0, keepdims=True)
            acc[q] = acc[q] * shrink + jnp.dot(
                vb[origin], e.astype(BF16), preferred_element_type=F32
            )
            return carry

        lax.fori_loop(0, 4, tile, 0)

    attend(z)

    out_ring1.forward()
    rings[3].own()
    rings2[1].own()
    rings2[3].own()

    def kv_step(step):
        for piece in (0, 1):
            for way in (0, 1):
                kv_arrived(step, way, piece)
                if step < 2 or (step == 2 and piece == way):
                    kv_send(step + 1, way, piece)

    kv_step(0)
    attend(at_z(-1))
    attend(at_z(1))
    out_ring1.far()
    rings2[2].own()
    kv_step(1)
    attend(at_z(-2))
    attend(at_z(2))
    rings2[1].forward()
    rings2[3].forward()
    rings[2].forward()
    rings[2].far()
    project(2)
    for i in range(NX):
        r = slice(i * 128, i * 128 + 128)
        u = rope(proj[r, 0:128], cosr[r, :], sinr[r, :], 64) * (128 ** -0.5)
        rk[r, :] = u.astype(BF16)
        rv[r, :] = proj[r, 128:256].astype(BF16)
    end = dz[z][0:1, :]
    forward_state = jnp.zeros((128, 128), F32)
    backward_state = jnp.zeros((128, 128), F32)
    for i in range(NX):
        r = slice(i * 128, i * 128 + 128)
        key = rk[r, :].astype(F32)
        value = rv[r, :]
        level = gcol[r, :]
        a = (key * jnp.exp(end - level)).T.astype(BF16)
        b = (key * jnp.exp(level)).T.astype(BF16)
        forward_state += jnp.dot(a, value, preferred_element_type=F32)
        backward_state += jnp.dot(b, value, preferred_element_type=F32)
    st[z, 0] = forward_state.astype(BF16)
    st[z, 1] = backward_state.astype(BF16)

    def st_send(step, way):
        origin = at_z(-step if way == 0 else step)
        device = along_z(zr if way == 0 else zl)
        base = ST + 4 * step + 2 * way
        states = st.at[origin] if step < 3 else st.at[origin, way]
        send(base, states, states, device)
        if step < 3 or way == 1:
            send(base + 1, dz.at[origin], dz.at[origin], device)

    def st_step(step):
        for way in (0, 1):
            origin = at_z(-(step + 1) if way == 0 else step + 1)
            base = ST + 4 * step + 2 * way
            arrived(base, st.at[origin] if step < 3 else st.at[origin, way])
            if step < 3 or way == 1:
                arrived(base + 1, dz.at[origin])
            if step < 3:
                st_send(step + 1, way)

    st_send(0, 0)
    st_send(0, 1)

    kv_step(2)
    attend(at_z(-3))
    rings[3].forward()
    rings2[2].forward()
    attend(at_z(3))
    st_step(0)

    for i in range(NX):
        r = slice(i * 128, i * 128 + 128)
        s = lax.dot_general(rq[r, :], rk[...], (((1,), (1,)), ((), ())), preferred_element_type=F32)
        level = jnp.concatenate([gcol[r, :]] * 4, axis=1)
        w = (s * jnp.exp(-jnp.abs(level - grow[...]))).astype(BF16)
        mix[i] = jnp.dot(w, rv[...], preferred_element_type=F32)

    st_step(1)
    rings[3].far()
    project(3)
    for i in range(NX):
        gate[i] = proj[i * 128 : i * 128 + 128, 0:128].astype(BF16)
    for d in (1, 2, 3):
        send(GT + d - 1, gate.at[xs[d]], gt.at[x], along_x(xs[d]))
    gt[x] = gate[x]

    st_step(2)
    kv_arrived(3, 0, 0)
    kv_arrived(3, 1, 1)
    attend(at_z(4))

    lam = par[3:4, 0:1]
    dgain = par[2:3, :]
    for t in range(2):
        first = acc[t] / l_run[t]
        second = acc[2 + t] / l_run[2 + t]
        both = first - lam * second
        both = both * lax.rsqrt(jnp.mean(both * both, axis=0, keepdims=True) + EPS)
        for h in range(2):
            feat[2 * t + h] = (both[:, h * 128 : h * 128 + 128].T * dgain).astype(BF16)
    for d in (1, 2, 3):
        send(DF + d - 1, feat.at[xs[d]], df.at[x], along_x(xs[d]))
    df[x] = feat[x]

    st_step(3)
    forward_state = jnp.zeros((128, 128), F32)
    total = jnp.zeros((1, 128), F32)
    for k in range(NZ - 1, -1, -1):
        take = jnp.where(k < z, 1.0, 0.0)
        forward_state += (jnp.exp(total) * take) * st[k, 0].astype(F32)
        total += dz[k][0:1, :] * take
    backward_state = jnp.zeros((128, 128), F32)
    total = jnp.zeros((1, 128), F32)
    for k in range(NZ):
        take = jnp.where(k > z, 1.0, 0.0)
        backward_state += (jnp.exp(total) * take) * st[k, 1].astype(F32)
        total += dz[k][0:1, :] * take
    states = jnp.concatenate([forward_state, backward_state], axis=0).astype(BF16)
    for i in range(NX):
        r = slice(i * 128, i * 128 + 128)
        query = rq[r, :].astype(F32)
        level = gcol[r, :]
        q2 = jnp.concatenate(
            [(query * jnp.exp(level)).astype(BF16), (query * jnp.exp(end - level)).astype(BF16)],
            axis=1,
        )
        mix[i] = mix[i] + jnp.dot(q2, states, preferred_element_type=F32)
    for d in (1, 2, 3):
        send(RM + d - 1, mix.at[xs[d]], rm.at[x], along_x(xs[d]))
    rm[x] = mix[x]

    for k in (1, 3, 2):
        rings2[k].far()
    for d in (1, 2, 3):
        arrived(GT + d - 1, gt.at[xs[4 - d]])
        arrived(DF + d - 1, df.at[xs[4 - d]])
        arrived(RM + d - 1, rm.at[xs[4 - d]])
    for h in range(2):
        a, b = rm[2 * h], rm[2 * h + 1]
        total = jnp.sum(a * a, axis=-1, keepdims=True) + jnp.sum(b * b, axis=-1, keepdims=True)
        scale = lax.rsqrt(total / 256 + EPS)
        for k, m in ((2 * h, a), (2 * h + 1, b)):
            g = gt[k].astype(F32)
            value = (g * jax.nn.sigmoid(g)) * (m * scale * par[4 + k : 5 + k, :])
            fall[:, k * 256 : k * 256 + 128] = value.astype(BF16)
            fall[:, k * 256 + 128 : k * 256 + 256] = df[k]

    mine = pl.ds(pl.multiple_of(c * 64, 64), 64)
    theirs = pl.ds(pl.multiple_of(other * 64, 64), 64)
    for k in range(NY):
        w = wo[k].reshape(1024, 512)
        part[k] = jnp.dot(fall[...], w, preferred_element_type=F32).astype(BF16)
        send(OUT + k, part.at[k, theirs], pin.at[k], partner)
    for k in range(NY):
        arrived(OUT + k, pin.at[k])
        value = part[k, mine, :].astype(F32) + pin[k].astype(F32)
        out[0, :, k * 512 : k * 512 + 512] = value.astype(BF16)
    for copy in sent:
        copy.wait_send()


def body(
    tokens, norm_gain, retain_query, retain_key, retain_value, retain_gate, differ_query,
    differ_key, differ_value, log_decay, lambdas, query_gain, key_gain, retain_gain,
    differ_gain, retain_out, differ_out,
):
    x = lax.axis_index("sp") % NX
    own = lambda a: lax.dynamic_slice_in_dim(a, x, 1, 0)
    par = jnp.concatenate(
        [
            own(query_gain.reshape(4, 128)),
            own(key_gain.reshape(4, 128)),
            own(differ_gain.reshape(4, 128)),
            own(jnp.broadcast_to(lambdas[:, None], (4, 128))),
            retain_gain.reshape(4, 128),
        ],
        axis=0,
    )
    dec = jnp.pad(log_decay[0].T, ((0, 6), (0, 0)))
    tab = jnp.asarray(rope_tables())
    anywhere = pl.BlockSpec(memory_space=pl.ANY)
    vmem = pl.BlockSpec(memory_space=pltpu.VMEM)
    V = pltpu.VMEM
    return pl.pallas_call(
        kernel,
        out_shape=jax.ShapeDtypeStruct((1, 64, D), BF16),
        in_specs=[anywhere] * 10 + [vmem] * 4,
        out_specs=vmem,
        scratch_shapes=[
            V((NX, 2, 128, 1024), BF16),
            V((BLOCK, D), BF16),
            V((D, 256), BF16), V((D, 256), BF16), V((D, 256), BF16), V((D, 128), BF16),
            V((NY, NX, 256, 512), BF16),
            V((NX, 8, 128), F32),
            V((NZ, BLOCK, 128), BF16),
            V((NZ, 128, BLOCK), BF16),
            V((NZ, 2, 128, 128), BF16),
            V((NZ, 8, 128), F32),
            V((BLOCK, 128), F32), V((BLOCK, 128), F32), V((BLOCK, 128), F32), V((BLOCK, 128), F32),
            V((BLOCK, 256), F32),
            V((4, 128, 256), BF16),
            V((4, 1, 256), F32), V((4, 1, 256), F32), V((4, 128, 256), F32),
            V((BLOCK, 128), BF16), V((BLOCK, 128), BF16), V((BLOCK, 128), BF16),
            V((1, BLOCK), F32), V((BLOCK, 128), F32),
            V((NX, 128, 128), F32),
            V((NX, 128, 128), BF16), V((NX, 128, 128), BF16),
            V((NX, 128, 128), BF16), V((NX, 128, 128), BF16), V((NX, 128, 128), F32),
            V((128, 1024), BF16),
            V((NY, 128, 512), BF16), V((NY, 64, 512), BF16),
            pltpu.SemaphoreType.DMA((COPIES,)),
            pltpu.SemaphoreType.DMA((COPIES,)),
            pltpu.SemaphoreType.DMA((LOCALS,)),
        ],
        compiler_params=pltpu.CompilerParams(
            collective_id=0, has_side_effects=True, vmem_limit_bytes=48 * 1024 * 1024
        ),
    )(
        tokens, retain_query, retain_key, retain_value, retain_gate, differ_query, differ_key,
        differ_value, retain_out, differ_out, dec, par, norm_gain.reshape(1, D), tab,
    )


def solution(mesh):
    in_specs = (
        P("fs", "sp", "tp"), P(),
        P("fs", "tp"), P("fs", "tp"), P("fs", "tp"), P("fs", "tp"), P("fs", "tp"), P("fs", "tp"), P("fs", "tp"),
        P("fs", "sp", "tp"),
        P("tp"), P("tp", None, None), P("tp", None, None), P("tp"), P("tp"),
        P("tp", "fs"), P("tp", "fs"),
    )
    out_specs = P("fs", ("sp", "tp"), None)
    return jax.shard_map(body, mesh=mesh, in_specs=in_specs, out_specs=out_specs, check_vma=False)
```

time: 371 us -> 104 us (0.28)
  waiting for transfers between devices: 188 us -> 0 us
  Pallas kernels: 0 us -> 86.7 us
  local copies, waits for them, and re-layouts: 77.4 us -> 16.5 us
  matrix products: 37.7 us -> 0 us
  other arithmetic: 25.9 us -> 0 us
  starting transfers between devices: 14 us -> 0 us
  between operations: 13.8 us -> 0.04 us
  blocking collectives: 11.7 us -> 0 us
    all_gather x3 -> x0, waiting for transfers between devices: 113 us -> none  [sent_together(): lax.all_gather(both, axis, axis=dim, tiled=True)]
    pallas_call x0 -> x1, Pallas kernels: none -> 86.7 us  [body(): pl.pallas_call(kernel, out_shape=jax.ShapeDtypeStruct((1, 64, D), BF16),...]
    reduce_scatter x1 -> x0, waiting for transfers between devices: 66.3 us -> none  [body(): lax.psum_scatter(jnp.dot(spread, joined, preferred_element_type=jnp.float...]
    dot_general x16 -> x0, matrix products: 37.7 us -> none  [the longest x4 16 us: absorb_block(): jnp.einsum('qhmd,khmd->mhqk', query_heads, key_block, preferred_element_t...]
    reshape x6 -> x2, local copies, waits for them, and re-layouts: 23.3 us -> 0.16 us  [the longest x1 0.08 us: body(): query_gain.reshape(4, 128)]
    convert_element_type x10 -> x0, other arithmetic: 13.9 us -> none  [the longest x4 12.3 us: absorb_block(): exponent.astype(jnp.bfloat16)]
    all_to_all x2 -> x0, starting transfers between devices: 13.7 us -> none  [the longest x1 9.55 us: sent_to_all(): return lax.all_to_all(copies, axis, split_axis=0, concat_axis=0, tiled=True)]
    unnamed x42 -> x35, local copies, waits for them, and re-layouts: 26.6 us -> 14.3 us
  transfers between devices with their start and end apart: 6 -> 0, of which waited for: 5 -> 0; matrix products, arithmetic and copies ran while one was open for 33% -> 0% of each run, Pallas kernels for 0% -> 0%
where the time goes in v1:
time: 104 us; the launch traced here: 103 us
  Pallas kernels  86.7 us (83%)
  local copies, waits for them, and re-layouts  16.5 us (16%)
    pallas_call x1, Pallas kernels, body(): pl.pallas_call(kernel, out_shape=jax.ShapeDtypeStruct((1, 64, D), BF16),...  86.7 us
    unnamed x35, local copies, waits for them, and re-layouts  14.3 us

profile of v1, /device:TPU:1, one launch (start us, length us, event | category | flops | bytes accessed | tf_op | source)
XLA Modules:
  0.0 103.3 jit_solution(15047406440290421332)
XLA Ops:
  0.0 0.0 copy-start.16
  0.0 0.7 copy-done.16
  0.7 0.6 dynamic_slice.17
  1.2 0.0 copy-start.12
  1.2 0.7 broadcast_in_dim.2
  1.9 0.0 copy-done.12
  1.9 0.0 copy-start.13
  1.9 0.1 reshape.18
  2.0 0.6 copy-done.13
  2.6 0.1 reshape.19
  2.7 0.7 constant_dynamic-slice_fusion
  3.4 0.0 copy-start.14
  3.4 0.0 copy-start.11
  3.4 0.7 copy-done.14
  4.1 0.0 copy-start.15
  4.1 0.7 copy-done.15
  4.7 0.0 copy-done.11
  4.8 0.0 copy-start
  4.8 1.0 %copy-done = bf16[512,512]{1,0:T(8,128)(2,1)S(1)} copy-done((bf16[512,512]{1,0:T(8,128)(2,1)S(1)}, bf16[512,512]{1,0:T(8,128)(2,1)}, u32[]{:S(2)}) %copy-start) | copy-done | bytes 524312
  5.8 0.0 copy-start.1
  5.8 1.0 %copy-done.1 = bf16[512,512]{1,0:T(8,128)(2,1)S(1)} copy-done((bf16[512,512]{1,0:T(8,128)(2,1)S(1)}, bf16[512,512]{1,0:T(8,128)(2,1)}, u32[]{:S(2)}) %copy-start.1) | copy-done | bytes 524312
  6.8 0.0 copy-start.2
  6.8 1.0 %copy-done.2 = bf16[512,512]{1,0:T(8,128)(2,1)S(1)} copy-done((bf16[512,512]{1,0:T(8,128)(2,1)S(1)}, bf16[512,512]{1,0:T(8,128)(2,1)}, u32[]{:S(2)}) %copy-start.2) | copy-done | bytes 524312
  7.9 0.0 copy-start.3
  7.9 1.0 %copy-done.3 = bf16[512,512]{1,0:T(8,128)(2,1)S(1)} copy-done((bf16[512,512]{1,0:T(8,128)(2,1)S(1)}, bf16[512,512]{1,0:T(8,128)(2,1)}, u32[]{:S(2)}) %copy-start.3) | copy-done | bytes 524312
  8.9 0.0 copy-start.4
  8.9 1.0 %copy-done.4 = bf16[512,512]{1,0:T(8,128)(2,1)S(1)} copy-done((bf16[512,512]{1,0:T(8,128)(2,1)S(1)}, bf16[512,512]{1,0:T(8,128)(2,1)}, u32[]{:S(2)}) %copy-start.4) | copy-done | bytes 524312
  10.0 0.0 copy-start.5
  10.0 1.0 %copy-done.5 = bf16[512,512]{1,0:T(8,128)(2,1)S(1)} copy-done((bf16[512,512]{1,0:T(8,128)(2,1)S(1)}, bf16[512,512]{1,0:T(8,128)(2,1)}, u32[]{:S(2)}) %copy-start.5) | copy-done | bytes 524312
  11.0 0.0 copy-start.6
  11.0 1.0 %copy-done.6 = bf16[512,512]{1,0:T(8,128)(2,1)S(1)} copy-done((bf16[512,512]{1,0:T(8,128)(2,1)S(1)}, bf16[512,512]{1,0:T(8,128)(2,1)}, u32[]{:S(2)}) %copy-start.6) | copy-done | bytes 524312
  12.0 0.0 copy-start.7
  12.0 0.9 copy-done.7
  13.0 0.0 copy-start.8
  13.0 0.9 copy-done.8
  13.9 0.0 copy-start.9
  13.9 0.9 copy-done.9
  14.9 0.0 copy-start.10
  14.9 0.9 copy-done.10
  15.8 86.7 %shard_map.172 = bf16[1,64,2048]{2,1,0:T(8,128)(2,1)S(1)} custom-call(bf16[1,128,1024]{2,1,0:T(8,128)(2,1)S(1)} %copy-done.7, bf16[512,256]{1,0:T(8,128)(2,1)S(1)} %copy-done.8, bf16[512,256]{1,0:T(8,128)(2,1)S(1)} %copy-done.9, bf16[512,512]{1,0:T(8,128)(2,1)S(1)} %copy-done, bf16[512,512]{1,0:T(8,128)(2,1)S(1)} %copy-done.1, ...), custom_call_target="tpu_custom_call" | custom-call | tf_op jit(solution)/shard_map/pallas_call | solution.py:525
  102.6 0.7 copy.20
  (3 shorter events, 0.0 us)
Async XLA Ops:
  0.0 0.7 copy-start.16
  1.2 0.7 copy-start.12
  1.9 0.7 copy-start.13
  3.4 0.7 copy-start.14
  3.4 1.4 %copy-start.11 = (f32[2048]{0:T(1024)S(1)}, f32[2048]{0:T(1024)}, u32[]{:S(2)}) copy-start(f32[2048]{0:T(1024)} %param.19) | copy-start | bytes 24580
  4.1 0.7 copy-start.15
  4.8 1.0 %copy-start = (bf16[512,512]{1,0:T(8,128)(2,1)S(1)}, bf16[512,512]{1,0:T(8,128)(2,1)}, u32[]{:S(2)}) copy-start(bf16[512,512]{1,0:T(8,128)(2,1)} %w_rv.1) | copy-start | bytes 1572868
  5.8 1.0 %copy-start.1 = (bf16[512,512]{1,0:T(8,128)(2,1)S(1)}, bf16[512,512]{1,0:T(8,128)(2,1)}, u32[]{:S(2)}) copy-start(bf16[512,512]{1,0:T(8,128)(2,1)} %w_rg.1) | copy-start | bytes 1572868
  6.8 1.0 %copy-start.2 = (bf16[512,512]{1,0:T(8,128)(2,1)S(1)}, bf16[512,512]{1,0:T(8,128)(2,1)}, u32[]{:S(2)}) copy-start(bf16[512,512]{1,0:T(8,128)(2,1)} %w_dq.1) | copy-start | bytes 1572868
  7.9 1.0 %copy-start.3 = (bf16[512,512]{1,0:T(8,128)(2,1)S(1)}, bf16[512,512]{1,0:T(8,128)(2,1)}, u32[]{:S(2)}) copy-start(bf16[512,512]{1,0:T(8,128)(2,1)} %w_dk.1) | copy-start | bytes 1572868
  8.9 1.0 %copy-start.4 = (bf16[512,512]{1,0:T(8,128)(2,1)S(1)}, bf16[512,512]{1,0:T(8,128)(2,1)}, u32[]{:S(2)}) copy-start(bf16[512,512]{1,0:T(8,128)(2,1)} %w_dv.1) | copy-start | bytes 1572868
  10.0 1.0 %copy-start.5 = (bf16[512,512]{1,0:T(8,128)(2,1)S(1)}, bf16[512,512]{1,0:T(8,128)(2,1)}, u32[]{:S(2)}) copy-start(bf16[512,512]{1,0:T(8,128)(2,1)} %w_ro.1) | copy-start | bytes 1572868
  11.0 1.0 %copy-start.6 = (bf16[512,512]{1,0:T(8,128)(2,1)S(1)}, bf16[512,512]{1,0:T(8,128)(2,1)}, u32[]{:S(2)}) copy-start(bf16[512,512]{1,0:T(8,128)(2,1)} %w_do.1) | copy-start | bytes 1572868
  12.0 0.9 copy-start.7
  13.0 0.9 copy-start.8
  13.9 0.9 copy-start.9
  14.9 0.9 copy-start.10

commit v2 on v1

v2 whole, which is shorter than its diff:
```python
import functools

import numpy as np
import jax
import jax.numpy as jnp
from jax import lax
from jax.experimental import pallas as pl
from jax.experimental.pallas import tpu as pltpu
from jax.sharding import PartitionSpec as P

F32 = jnp.float32
BF16 = jnp.bfloat16
MESH = pl.DeviceIdType.MESH
EPS = 1e-06
ROPE_BASE = 10000.0
NX, NY, NZ = 4, 4, 8
ROWS = 128
BLOCK = NX * ROWS
D = 2048
WIDTHS = (256, 256, 256, 128)

TOK = 0
PART = 8
W0 = 16
W1 = 24
W2 = 28
W3 = 32
OY = 36
OZ = 40
OX = 48
DEC = 56
KV = 59
ST = 75
DF = 91
GT = 94
RM = 97
OUT = 100
COPIES = 104
LOCALS = 24


def rope_tables():
    lane = np.arange(128)
    value = np.arange(64, dtype=np.float64)[:, None]
    tables = []
    for group in (32, 64):
        inverse = ROPE_BASE ** (-2.0 * ((lane % group) % (group // 2)) / group)
        angle = value * inverse[None, :]
        sign = np.where((lane % group) < group // 2, -1.0, 1.0)[None, :]
        tables += [np.cos(angle), np.sin(angle) * sign]
    return np.stack(tables).astype(np.float32)


class Phases:
    def __init__(self):
        self.scope = None

    def __call__(self, name):
        if self.scope is not None:
            self.scope.__exit__(None, None, None)
        self.scope = jax.named_scope(name) if name else None
        if self.scope is not None:
            self.scope.__enter__()


def kernel(
    tok_in, w_rq, w_rk, w_rv, w_rg, w_dq, w_dk, w_dv, w_ro, w_do,
    dec_hbm, lam_hbm, qgain_hbm, kgain_hbm, rgain_hbm, dgain_hbm, ngain_hbm, tab_hbm,
    out,
    dec_in, lam_in, qgain_in, kgain_in, rgain_in, dgain_in, gain_in, tab, tok, xn, wg0, wg1, wg2, wg3, wo, dec, kb, vb, st, dz, cosd, sind, cosr, sinr, proj, qbd,
    m_run, l_run, acc, rq, rk, rv, grow, gcol, mix, gate, feat, df, gt, rm, fall, part, pin,
    ssem, rsem, lsem,
):
    phase = Phases()
    sp = lax.axis_index("sp")
    z, x = sp // NX, sp % NX
    y = lax.axis_index("fs")
    c = lax.axis_index("tp")
    other = 1 - c

    def along_x(i):
        return {"sp": z * NX + i}

    def along_y(i):
        return {"fs": i}

    def along_z(i):
        return {"sp": i * NX + x}

    partner = {"tp": other}
    xs = [x, (x + 1) % NX, (x + 2) % NX, (x + 3) % NX]
    ys = [y, (y + 1) % NY, (y + 2) % NY, (y + 3) % NY]
    zr, zl = (z + 1) % NZ, (z + NZ - 1) % NZ

    def remote(i, src, dst, device):
        return pltpu.make_async_remote_copy(
            src_ref=src, dst_ref=dst, send_sem=ssem.at[i], recv_sem=rsem.at[i],
            device_id=device, device_id_type=MESH,
        )

    sent = []

    def send(i, src, dst, device):
        copy = remote(i, src, dst, device)
        copy.start()
        sent.append(copy)

    def arrived(i, ref):
        remote(i, ref, ref, partner).wait_recv()

    class Ring4:
        def __init__(self, base, right, left, own, to_right, to_left, half, onward, far):
            self.base, self.right, self.left = base, right, left
            self.src, self.to_right, self.to_left, self.half = own, to_right, to_left, half
            self.onward, self.far_half = onward, far

        def own(self):
            send(self.base, self.src, self.to_right, self.right)
            send(self.base + 1, self.src, self.to_left, self.left)

        def near(self):
            self.from_left()
            self.from_right()

        def from_left(self):
            arrived(self.base, self.half[2])
            send(self.base + 2, self.half[0], self.onward[0], self.right)

        def from_right(self):
            arrived(self.base + 1, self.half[3])
            send(self.base + 3, self.half[1], self.onward[1], self.left)

        def far(self):
            arrived(self.base + 2, self.far_half[0])
            arrived(self.base + 3, self.far_half[1])

    def ring_at(base, at, sides, full, half):
        return Ring4(
            base, sides[0], sides[1], full(at[0]), full(at[0]), full(at[0]),
            (half(at[3], 0), half(at[1], 1), full(at[3]), full(at[1])),
            (half(at[3], 0), half(at[1], 1)), (half(at[2], 0), half(at[2], 1)),
        )

    wgs = (wg0, wg1, wg2, wg3)
    def rows_of(start, size):
        return pl.ds(pl.multiple_of(start, size & -size), size)

    token_rings = [
        ring_at(
            TOK + 4 * piece, xs, (along_x(xs[1]), along_x(xs[3])),
            lambda i, p=piece: tok.at[i, c, pl.ds(p * 64, 64)],
            lambda i, h, p=piece: tok.at[i, c, pl.ds(p * 64 + h * 32, 32)],
        )
        for piece in (0, 1)
    ]

    def weight_ring(base, ref, start, size):
        return ring_at(
            base, ys, (along_y(ys[1]), along_y(ys[3])),
            lambda i: ref.at[rows_of(i * 512 + start, size)],
            lambda i, h: ref.at[rows_of(i * 512 + start + h * (size // 2), size // 2)],
        )

    ring0 = [weight_ring(W0 + 4 * piece, wg0, piece * 256, 256) for piece in (0, 1)]
    ring1 = weight_ring(W1, wg1, 0, 512)
    ring2 = weight_ring(W2, wg2, 0, 512)
    ring3 = weight_ring(W3, wg3, 0, 512)

    zc = z % 4
    zcs = [(zc + d) % 4 for d in range(4)]

    def slice_of(slot, i, h=None):
        if h is None:
            return wo.at[slot, x, rows_of(i * 64, 64)]
        return wo.at[slot, x, rows_of(i * 64 + h * 32, 32)]

    out_y = Ring4(
        OY, along_y(ys[1]), along_y(ys[3]), slice_of(0, zc), slice_of(2, zc), slice_of(1, zc),
        (slice_of(2, zc, 0), slice_of(1, zc, 1), slice_of(2, zc), slice_of(1, zc)),
        (slice_of(3, zc, 0), slice_of(3, zc, 1)), (slice_of(3, zc, 0), slice_of(3, zc, 1)),
    )

    near, far = pl.ds(1, 2), 3
    out_z = []
    out_x = []
    for k, slot in enumerate((near, far)):
        piece = functools.partial(slice_of, slot)
        out_z.append(ring_at(OZ + 4 * k, zcs, (along_z(zr), along_z(zl)), piece, piece))
        out_x.append(
            ring_at(
                OX + 4 * k, xs, (along_x(xs[1]), along_x(xs[3])),
                lambda i, s=slot: wo.at[s, i],
                lambda i, h, s=slot: wo.at[s, i, pl.ds(h * 128, 128)],
            )
        )

    def local(i, src, dst):
        copy = pltpu.make_async_copy(src, dst, lsem.at[i])
        copy.start()
        return copy

    col = pl.ds(pl.multiple_of(x * 128, 128), 128)
    col2 = pl.ds(pl.multiple_of((x // 2) * 128, 128), 128)
    own_rows = pl.ds(pl.multiple_of(y * 512, 512), 512)
    lo, hi = pl.ds(0, 128), pl.ds(128, 128)
    load_tok = local(0, tok_in.at[0], tok.at[x, c])
    load_g = [
        [local(1, w_dk.at[:, col], wg0.at[own_rows, lo]), local(2, w_dv.at[:, col], wg0.at[own_rows, hi])],
        [local(3, w_dq.at[:, col], wg1.at[own_rows, lo]), local(4, w_rq.at[:, col2], wg1.at[own_rows, hi])],
        [local(5, w_rk.at[:, col2], wg2.at[own_rows, lo]), local(6, w_rv.at[:, col], wg2.at[own_rows, hi])],
        [local(7, w_rg.at[:, col], wg3.at[own_rows])],
    ]
    load_o = []
    for i in range(NX):
        load_o.append(local(8 + 2 * i, w_ro.at[pl.ds(i * 128, 128)], wo.at[0, i, lo]))
        load_o.append(local(9 + 2 * i, w_do.at[pl.ds(i * 128, 128)], wo.at[0, i, hi]))

    load_small = [
        local(16 + i, src, dst)
        for i, (src, dst) in enumerate((
            (dec_hbm, dec_in), (lam_hbm, lam_in), (qgain_hbm, qgain_in), (kgain_hbm, kgain_in),
            (rgain_hbm, rgain_in), (dgain_hbm, dgain_in), (ngain_hbm, gain_in), (tab_hbm, tab),
        ))
    ]

    phase("barrier")
    barrier = pltpu.get_barrier_semaphore()
    peers = [along_x(xs[1]), along_x(xs[2]), along_x(xs[3]), along_y(ys[1]), along_y(ys[3]),
             along_z(zr), along_z(zl), partner]
    for peer in peers:
        pl.semaphore_signal(barrier, inc=1, device_id=peer, device_id_type=MESH)
    pl.semaphore_wait(barrier, len(peers))

    phase("loads")
    load_tok.wait()
    for ring in token_rings:
        ring.own()
    send(PART, tok.at[x, c], tok.at[x, c], partner)
    for copy in load_g[0]:
        copy.wait()
    ring0[0].own()
    for copy in load_o:
        copy.wait()
    out_y.own()
    ring0[1].own()
    for copy in load_small:
        copy.wait()
    for d in (1, 2, 3):
        send(DEC + d - 1, dec_in, dec.at[x], along_x(xs[d]))
    dec[x] = dec_in[...]
    for group in load_g[1:]:
        for copy in group:
            copy.wait()

    lane = lax.broadcasted_iota(jnp.int32, (128, 128), 1)
    sub = lax.broadcasted_iota(jnp.int32, (128, 128), 0)

    phase("tables")
    lane64 = lax.broadcasted_iota(jnp.int32, (64, 128), 1)
    zrow = pl.ds(pl.multiple_of(z * 8, 8), 8)
    for k, ref in enumerate((cosd, sind, cosr, sinr)):
        by_row = tab[k, zrow, :]
        by_col = tab[k]
        is_row = (lane64 % 64) < 32 if k < 2 else lane64 < 64
        for b in range(8):
            ref[b * 64 : b * 64 + 64, :] = jnp.where(is_row, by_row[b : b + 1, :], by_col)

    def rope(u, cos, sin, group):
        half = group // 2
        up = pltpu.roll(u, 128 - half, 1)
        down = pltpu.roll(u, half, 1)
        return u * cos + jnp.where((lane % group) < half, up, down) * sin

    def map_norm(u, gain):
        square = u * u
        first = jnp.sum(jnp.where(lane < 64, square, 0.0), axis=-1, keepdims=True)
        second = jnp.sum(jnp.where(lane < 64, 0.0, square), axis=-1, keepdims=True)
        scale = jnp.where(
            lane < 64, lax.rsqrt(first / 64 + EPS), lax.rsqrt(second / 64 + EPS)
        )
        return u * scale * gain

    order = [xs[0], xs[3], xs[1], xs[2]]

    def block_rows(j):
        return rows_of(order[j] * 128, 128)

    def normalize(j):
        i = order[j]
        for k in range(8):
            r = slice(k * 16, k * 16 + 16)
            w = slice(j * 128 + k * 16, j * 128 + k * 16 + 16)
            a = tok[i, 0, r, :].astype(F32)
            b = tok[i, 1, r, :].astype(F32)
            total = jnp.sum(a * a, axis=-1, keepdims=True) + jnp.sum(b * b, axis=-1, keepdims=True)
            scale = lax.rsqrt(total / D + EPS)
            xn[w, 0:1024] = (a * scale * gain_in[:, 0:1024]).astype(BF16)
            xn[w, 1024:2048] = (b * scale * gain_in[:, 1024:2048]).astype(BF16)

    def project(g, start=0, size=BLOCK):
        ref = wgs[g]
        width = WIDTHS[g]
        step = 256 if size % 256 == 0 else 128
        for j in range(start, start + size, step):
            proj[j : j + step, 0:width] = jnp.dot(
                xn[j : j + step, :], ref[...], preferred_element_type=F32
            )

    def part_send(n, block, start, size):
        ref = tok.at[block, c, pl.ds(start, size)]
        send(PART + n, ref, ref, partner)

    def part_arrived(n, block, start, size):
        arrived(PART + n, tok.at[block, other, pl.ds(start, size)])

    kgain = jnp.concatenate([kgain_in[x][0:1, :], kgain_in[x][1:2, :]], axis=1)

    def keys_values(j):
        r = slice(j * 128, j * 128 + 128)
        a = block_rows(j)
        u = map_norm(proj[r, 0:128], kgain)
        kb[z, r, :] = rope(u, cosd[a, :], sind[a, :], 32).astype(BF16)
        vb[z, :, r] = proj[r, 128:256].T.astype(BF16)

    phase("w0a")
    ring0[0].near()
    phase("tok_a")
    token_rings[0].near()
    part_send(1, order[1], 0, 64)
    part_send(2, order[2], 0, 64)
    phase("oy")
    out_y.near()
    out_z[0].own()
    phase("w0b")
    ring0[1].near()
    ring1.own()
    phase("tok_b")
    token_rings[1].near()
    part_send(3, order[1], 64, 64)
    part_send(4, order[2], 64, 64)
    phase("norm0")
    arrived(PART, tok.at[x, other])
    normalize(0)
    phase("norm1")
    part_arrived(1, order[1], 0, 64)
    part_arrived(3, order[1], 64, 64)
    normalize(1)
    phase("tok_far_a")
    token_rings[0].far()
    part_send(5, order[3], 0, 64)
    phase("oz_near")
    out_z[0].near()
    phase("norm2")
    part_arrived(2, order[2], 0, 64)
    part_arrived(4, order[2], 64, 64)
    normalize(2)
    phase("tok_far_b")
    token_rings[1].far()
    part_send(6, order[3], 64, 64)
    phase("oy_far")
    out_y.far()
    out_z[1].own()
    phase("w0_far")
    ring0[0].far()
    ring0[1].far()
    phase("project0")
    project(0, 0, 384)
    phase("kv_post")
    for j in range(3):
        keys_values(j)
    phase("norm3")
    part_arrived(5, order[3], 0, 64)
    part_arrived(6, order[3], 64, 64)
    normalize(3)
    phase("project0b")
    project(0, 384, 128)
    keys_values(3)

    zs = [(z + NZ + d) % NZ for d in range(-4, 5)]

    def at_z(d):
        return zs[d + 4]

    def kv_send(step, way, piece):
        origin = at_z(-step if way == 0 else step)
        ref = (kb, vb)[piece].at[origin]
        send(KV + 4 * step + 2 * way + piece, ref, ref, along_z(zr if way == 0 else zl))

    def kv_arrived(step, way, piece):
        origin = at_z(-(step + 1) if way == 0 else step + 1)
        arrived(KV + 4 * step + 2 * way + piece, (kb, vb)[piece].at[origin])

    for piece in (0, 1):
        for way in (0, 1):
            kv_send(0, way, piece)

    phase("levels")
    for d in (1, 2, 3):
        arrived(DEC + d - 1, dec.at[xs[4 - d]])
    lane8 = lax.broadcasted_iota(jnp.int32, (2, 128), 1)
    offset = jnp.zeros((1, 1), F32)
    head = x // 2
    for b in range(NX):
        level = dec[b]
        for k in (1, 2, 4, 8, 16, 32, 64):
            level = level + jnp.where(lane8 >= k, pltpu.roll(level, k, 1), 0.0)
        row = jnp.where(head == 0, level[0:1, :], level[1:2, :]) + offset
        offset = row[:, 127:128]
        grow[:, b * 128 : b * 128 + 128] = row
        gcol[b * 128 : b * 128 + 128, :] = jnp.broadcast_to(row, (128, 128)).T
    dz[z] = jnp.broadcast_to(offset, (8, 128))

    phase("oz_near_far")
    out_z[0].far()
    out_x[0].own()
    out_z[1].near()
    phase("w1")
    ring1.near()
    ring2.own()
    phase("oz_far_far")
    out_z[1].far()
    out_x[1].own()

    def kv_step(step):
        for piece in (0, 1):
            for way in (0, 1):
                kv_arrived(step, way, piece)
                if step < 2 or (step == 2 and piece == way):
                    kv_send(step + 1, way, piece)

    phase("w1_far")
    ring1.far()
    phase("project1")
    project(1)
    phase("q_post")
    qgain = jnp.concatenate([qgain_in[x][0:1, :], qgain_in[x][1:2, :]], axis=1)
    for i in range(NX):
        r = slice(i * 128, i * 128 + 128)
        a = block_rows(i)
        u = map_norm(proj[r, 0:128], qgain)
        u = rope(u, cosd[a, :], sind[a, :], 32).astype(BF16).astype(F32) * 0.125
        u = u.T
        s = slice((i % 2) * 128, (i % 2) * 128 + 128)
        qbd[i // 2, :, s] = jnp.where(sub < 64, u, 0.0).astype(BF16)
        qbd[2 + i // 2, :, s] = jnp.where(sub < 64, 0.0, u).astype(BF16)
        rq[a, :] = rope(proj[r, 128:256], cosr[a, :], sinr[a, :], 64).astype(BF16)

    m_run[...] = jnp.full((4, 1, 256), -jnp.inf, F32)
    l_run[...] = jnp.zeros((4, 1, 256), F32)
    acc[...] = jnp.zeros((4, 128, 256), F32)

    def attend(*origins):
        for q in range(4):
            s = [jnp.dot(kb[o], qbd[q], preferred_element_type=F32) for o in origins]
            before = m_run[q]
            now = before
            for part_s in s:
                now = jnp.maximum(now, jnp.max(part_s, axis=0, keepdims=True))
            shrink = jnp.exp(before - now)
            m_run[q] = now
            total = l_run[q] * shrink
            value = acc[q] * shrink
            for o, part_s in zip(origins, s):
                e = jnp.exp(part_s - now)
                total = total + jnp.sum(e, axis=0, keepdims=True)
                value = value + jnp.dot(vb[o], e.astype(BF16), preferred_element_type=F32)
            l_run[q] = total
            acc[q] = value

    phase("kv_step0")
    kv_step(0)
    phase("attend0")
    attend(z)
    phase("w2")
    ring2.near()
    ring3.own()
    phase("attend1")
    attend(at_z(-1), at_z(1))
    phase("kv_step1")
    kv_step(1)
    phase("attend2")
    attend(at_z(-2), at_z(2))
    phase("ox_near")
    out_x[0].near()
    phase("w2_far")
    ring2.far()
    phase("project2")
    project(2)
    phase("states")
    for i in range(NX):
        r = slice(i * 128, i * 128 + 128)
        a = block_rows(i)
        u = rope(proj[r, 0:128], cosr[a, :], sinr[a, :], 64) * (128 ** -0.5)
        rk[a, :] = u.astype(BF16)
        rv[a, :] = proj[r, 128:256].astype(BF16)
    end = dz[z][0:1, :]
    forward_state = jnp.zeros((128, 128), F32)
    backward_state = jnp.zeros((128, 128), F32)
    for i in range(NX):
        r = slice(i * 128, i * 128 + 128)
        key = rk[r, :].astype(F32)
        value = rv[r, :]
        level = gcol[r, :]
        a = (key * jnp.exp(end - level)).T.astype(BF16)
        b = (key * jnp.exp(level)).T.astype(BF16)
        forward_state += jnp.dot(a, value, preferred_element_type=F32)
        backward_state += jnp.dot(b, value, preferred_element_type=F32)
    st[z, 0] = forward_state.astype(BF16)
    st[z, 1] = backward_state.astype(BF16)

    def st_send(step, way):
        origin = at_z(-step if way == 0 else step)
        device = along_z(zr if way == 0 else zl)
        base = ST + 4 * step + 2 * way
        states = st.at[origin] if step < 3 else st.at[origin, way]
        send(base, states, states, device)
        if step < 3 or way == 1:
            send(base + 1, dz.at[origin], dz.at[origin], device)

    def st_step(step):
        for way in (0, 1):
            origin = at_z(-(step + 1) if way == 0 else step + 1)
            base = ST + 4 * step + 2 * way
            arrived(base, st.at[origin] if step < 3 else st.at[origin, way])
            if step < 3 or way == 1:
                arrived(base + 1, dz.at[origin])
            if step < 3:
                st_send(step + 1, way)

    st_send(0, 0)
    st_send(0, 1)

    phase("w3")
    ring3.near()
    phase("kv_step2")
    kv_step(2)
    phase("attend3")
    attend(at_z(-3), at_z(3))
    phase("st_step0")
    st_step(0)
    phase("ox_far")
    out_x[1].near()
    phase("intra")
    for i in range(NX):
        r = slice(i * 128, i * 128 + 128)
        s = lax.dot_general(rq[r, :], rk[...], (((1,), (1,)), ((), ())), preferred_element_type=F32)
        level = jnp.concatenate([gcol[r, :]] * 4, axis=1)
        w = (s * jnp.exp(-jnp.abs(level - grow[...]))).astype(BF16)
        mix[i] = jnp.dot(w, rv[...], preferred_element_type=F32)

    phase("st_step1")
    st_step(1)
    phase("w3_far")
    ring3.far()
    phase("gate")
    project(3)
    for i in range(NX):
        gate[i] = proj[i * 128 : i * 128 + 128, 0:128].astype(BF16)
    for d, j in ((1, 2), (2, 3), (3, 1)):
        send(GT + d - 1, gate.at[j], gt.at[x], along_x(xs[d]))
    gt[x] = gate[0]

    phase("st_step2")
    st_step(2)
    phase("kv_last")
    kv_arrived(3, 0, 0)
    kv_arrived(3, 1, 1)
    phase("attend4")
    attend(at_z(4))
    phase("diff_out")

    lane4 = lax.broadcasted_iota(jnp.int32, (1, 4), 1)
    lam = jnp.sum(jnp.where(lane4 == x, lam_in[...], 0.0), axis=-1, keepdims=True)
    dgain = dgain_in[pl.ds(x, 1), :]
    for t in range(2):
        first = acc[t] / l_run[t]
        second = acc[2 + t] / l_run[2 + t]
        both = first - lam * second
        both = both * lax.rsqrt(jnp.mean(both * both, axis=0, keepdims=True) + EPS)
        for h in range(2):
            feat[2 * t + h] = (both[:, h * 128 : h * 128 + 128].T * dgain).astype(BF16)
    for d, j in ((1, 2), (2, 3), (3, 1)):
        send(DF + d - 1, feat.at[j], df.at[x], along_x(xs[d]))
    df[x] = feat[0]

    phase("st_step3")
    st_step(3)
    phase("carried")
    forward_state = jnp.zeros((128, 128), F32)
    total = jnp.zeros((1, 128), F32)
    for k in range(NZ - 1, -1, -1):
        take = jnp.where(k < z, 1.0, 0.0)
        forward_state += (jnp.exp(total) * take) * st[k, 0].astype(F32)
        total += dz[k][0:1, :] * take
    backward_state = jnp.zeros((128, 128), F32)
    total = jnp.zeros((1, 128), F32)
    for k in range(NZ):
        take = jnp.where(k > z, 1.0, 0.0)
        backward_state += (jnp.exp(total) * take) * st[k, 1].astype(F32)
        total += dz[k][0:1, :] * take
    states = jnp.concatenate([forward_state, backward_state], axis=0).astype(BF16)
    for i in range(NX):
        r = slice(i * 128, i * 128 + 128)
        query = rq[r, :].astype(F32)
        level = gcol[r, :]
        q2 = jnp.concatenate(
            [(query * jnp.exp(level)).astype(BF16), (query * jnp.exp(end - level)).astype(BF16)],
            axis=1,
        )
        mix[i] = mix[i] + jnp.dot(q2, states, preferred_element_type=F32)
    for d in (1, 2, 3):
        send(RM + d - 1, mix.at[xs[d]], rm.at[x], along_x(xs[d]))
    rm[x] = mix[x]

    phase("o2_far")
    for ring in out_x:
        ring.far()
    phase("home_wait")
    for d in (1, 2, 3):
        arrived(GT + d - 1, gt.at[xs[4 - d]])
        arrived(DF + d - 1, df.at[xs[4 - d]])
        arrived(RM + d - 1, rm.at[xs[4 - d]])
    phase("home")
    for h in range(2):
        a, b = rm[2 * h], rm[2 * h + 1]
        total = jnp.sum(a * a, axis=-1, keepdims=True) + jnp.sum(b * b, axis=-1, keepdims=True)
        scale = lax.rsqrt(total / 256 + EPS)
        for k, m in ((2 * h, a), (2 * h + 1, b)):
            g = gt[k].astype(F32)
            value = (g * jax.nn.sigmoid(g)) * (m * scale * rgain_in[k : k + 1, :])
            fall[:, k * 256 : k * 256 + 128] = value.astype(BF16)
            fall[:, k * 256 + 128 : k * 256 + 256] = df[k]

    phase("out_dot")
    mine = pl.ds(pl.multiple_of(c * 64, 64), 64)
    theirs = pl.ds(pl.multiple_of(other * 64, 64), 64)
    for k in range(NY):
        w = wo[k].reshape(1024, 512)
        part[k] = jnp.dot(fall[...], w, preferred_element_type=F32).astype(BF16)
        send(OUT + k, part.at[k, theirs], pin.at[k], partner)
    phase("out_wait")
    for k in range(NY):
        arrived(OUT + k, pin.at[k])
        value = part[k, mine, :].astype(F32) + pin[k].astype(F32)
        out[0, :, rows_of(ys[(0, 1, 3, 2)[k]] * 512, 512)] = value.astype(BF16)
    phase("drain")
    for copy in sent:
        copy.wait_send()
    phase(None)


def body(
    tokens, norm_gain, retain_query, retain_key, retain_value, retain_gate, differ_query,
    differ_key, differ_value, log_decay, lambdas, query_gain, key_gain, retain_gain,
    differ_gain, retain_out, differ_out,
):
    hbm = pl.BlockSpec(memory_space=pltpu.HBM)
    vmem = pl.BlockSpec(memory_space=pltpu.VMEM)
    V = pltpu.VMEM
    return pl.pallas_call(
        kernel,
        out_shape=jax.ShapeDtypeStruct((1, 64, D), BF16),
        in_specs=[hbm] * 18,
        out_specs=vmem,
        scratch_shapes=[
            V((2, 128), F32), V((1, 4), F32), V((4, 2, 64), F32), V((4, 2, 64), F32),
            V((4, 128), F32), V((4, 128), F32), V((1, D), F32), V((4, 64, 128), F32),
            V((NX, 2, 128, 1024), BF16),
            V((BLOCK, D), BF16),
            V((D, 256), BF16), V((D, 256), BF16), V((D, 256), BF16), V((D, 128), BF16),
            V((NY, NX, 256, 512), BF16),
            V((NX, 2, 128), F32),
            V((NZ, BLOCK, 128), BF16),
            V((NZ, 128, BLOCK), BF16),
            V((NZ, 2, 128, 128), BF16),
            V((NZ, 8, 128), F32),
            V((BLOCK, 128), F32), V((BLOCK, 128), F32), V((BLOCK, 128), F32), V((BLOCK, 128), F32),
            V((BLOCK, 256), F32),
            V((4, 128, 256), BF16),
            V((4, 1, 256), F32), V((4, 1, 256), F32), V((4, 128, 256), F32),
            V((BLOCK, 128), BF16), V((BLOCK, 128), BF16), V((BLOCK, 128), BF16),
            V((1, BLOCK), F32), V((BLOCK, 128), F32),
            V((NX, 128, 128), F32),
            V((NX, 128, 128), BF16), V((NX, 128, 128), BF16),
            V((NX, 128, 128), BF16), V((NX, 128, 128), BF16), V((NX, 128, 128), F32),
            V((128, 1024), BF16),
            V((NY, 128, 512), BF16), V((NY, 64, 512), BF16),
            pltpu.SemaphoreType.DMA((COPIES,)),
            pltpu.SemaphoreType.DMA((COPIES,)),
            pltpu.SemaphoreType.DMA((LOCALS,)),
        ],
        compiler_params=pltpu.CompilerParams(
            collective_id=0, has_side_effects=True, vmem_limit_bytes=67000000
        ),
    )(
        tokens, retain_query, retain_key, retain_value, retain_gate, differ_query, differ_key,
        differ_value, retain_out, differ_out, log_decay[0].T, lambdas.reshape(1, 4), query_gain,
        key_gain, retain_gain.reshape(4, 128), differ_gain.reshape(4, 128), norm_gain.reshape(1, D),
        jnp.asarray(rope_tables()),
    )


def solution(mesh):
    in_specs = (
        P("fs", "sp", "tp"), P(),
        P("fs", "tp"), P("fs", "tp"), P("fs", "tp"), P("fs", "tp"), P("fs", "tp"), P("fs", "tp"), P("fs", "tp"),
        P("fs", "sp", "tp"),
        P("tp"), P("tp", None, None), P("tp", None, None), P("tp"), P("tp"),
        P("tp", "fs"), P("tp", "fs"),
    )
    out_specs = P("fs", ("sp", "tp"), None)
    return jax.shard_map(body, mesh=mesh, in_specs=in_specs, out_specs=out_specs, check_vma=False)
```

time: 104 us -> 75.7 us (0.73)
  local copies, waits for them, and re-layouts: 16.5 us -> 1.67 us
  Pallas kernels: 86.7 us -> 73.9 us
    pallas_call x1, Pallas kernels: 86.7 us -> 73.9 us  [body(): pl.pallas_call(kernel, out_shape=jax.ShapeDtypeStruct((1, 64, D), BF16),...]
    unnamed x35 -> x1, local copies, waits for them, and re-layouts: 14.3 us -> 1.67 us
    dynamic_slice x3 -> x0, local copies, waits for them, and re-layouts: 1.28 us -> none  [body(): own = lambda a: lax.dynamic_slice_in_dim(a, x, 1, 0)]
where the time goes in v2:
time: 75.7 us; the launch traced here: 75.6 us
  Pallas kernels  73.9 us (98%)
  local copies, waits for them, and re-layouts  1.67 us (2%)
    pallas_call x1, Pallas kernels, body(): pl.pallas_call(kernel, out_shape=jax.ShapeDtypeStruct((1, 64, D), BF16),...  73.9 us
    unnamed x1, local copies, waits for them, and re-layouts  1.67 us

profile of v2, /device:TPU:1, one launch (start us, length us, event | category | flops | bytes accessed | tf_op | source)
XLA Modules:
  0.0 75.6 jit_solution(10415666653920254321)
XLA Ops:
  0.0 73.9 %shard_map.172 = bf16[1,64,2048]{2,1,0:T(8,128)(2,1)} custom-call(bf16[1,128,1024]{2,1,0:T(8,128)(2,1)} %tok_in.1, bf16[512,256]{1,0:T(8,128)(2,1)} %w_rq.1, bf16[512,256]{1,0:T(8,128)(2,1)} %w_rk.1, bf16[512,512]{1,0:T(8,128)(2,1)} %w_rv.1, bf16[512,512]{1,0:T(8,128)(2,1)} %w_rg.1, bf16[512,512]{1,0:T(8,128)(2,1)} %w_dq.1, bf16[512,512]{1,0:T(8,128)(2,1)} %w_dk.1, ...), custom_call_target="tpu_custom_call" | custom-call | tf_op jit(solution)/shard_map/pallas_call | solution.py:660
  73.9 1.7 %copy.20 = bf16[1,64,2048]{2,1,0:T(8,128)(2,1)} copy(bf16[1,64,2048]{2,1,0:T(8,128)(2,1)} %shard_map.172) | data formatting | bytes 524288

commit v3 on v2

--- a/solution.py
+++ b/solution.py
@@ -17,7 +17,7 @@
 ROWS = 128
 BLOCK = NX * ROWS
 D = 2048
-WIDTHS = (256, 256, 256, 128)
+WIDTHS = (256, 256, 128, 256)
 
 TOK = 0
 PART = 8
@@ -67,8 +67,8 @@
     tok_in, w_rq, w_rk, w_rv, w_rg, w_dq, w_dk, w_dv, w_ro, w_do,
     dec_hbm, lam_hbm, qgain_hbm, kgain_hbm, rgain_hbm, dgain_hbm, ngain_hbm, tab_hbm,
     out,
-    dec_in, lam_in, qgain_in, kgain_in, rgain_in, dgain_in, gain_in, tab, tok, xn, wg0, wg1, wg2, wg3, wo, dec, kb, vb, st, dz, cosd, sind, cosr, sinr, proj, qbd,
-    m_run, l_run, acc, rq, rk, rv, grow, gcol, mix, gate, feat, df, gt, rm, fall, part, pin,
+    dec_in, lam_in, qgain_in, kgain_in, rgain_in, dgain_in, gain_in, tab, tok, xn, wg0, wg1, wg2, wg3, wo, dec, kb, vb, st, dz, cosd, sind, cosr, sinr, proj, proj2, qbd,
+    m_run, l_run, acc, rq, rk, rv, grow, gcol, mix, gate, feat, df, gt, rm, fall, part, pin, mixed, total_out,
     ssem, rsem, lsem,
 ):
     phase = Phases()
@@ -118,17 +118,17 @@
             send(self.base, self.src, self.to_right, self.right)
             send(self.base + 1, self.src, self.to_left, self.left)
 
+        def wait(self):
+            arrived(self.base, self.half[2])
+            arrived(self.base + 1, self.half[3])
+
+        def forward(self):
+            send(self.base + 2, self.half[0], self.onward[0], self.right)
+            send(self.base + 3, self.half[1], self.onward[1], self.left)
+
         def near(self):
-            self.from_left()
-            self.from_right()
-
-        def from_left(self):
-            arrived(self.base, self.half[2])
-            send(self.base + 2, self.half[0], self.onward[0], self.right)
-
-        def from_right(self):
-            arrived(self.base + 1, self.half[3])
-            send(self.base + 3, self.half[1], self.onward[1], self.left)
+            self.wait()
+            self.forward()
 
         def far(self):
             arrived(self.base + 2, self.far_half[0])
@@ -206,14 +206,14 @@
     load_tok = local(0, tok_in.at[0], tok.at[x, c])
     load_g = [
         [local(1, w_dk.at[:, col], wg0.at[own_rows, lo]), local(2, w_dv.at[:, col], wg0.at[own_rows, hi])],
-        [local(3, w_dq.at[:, col], wg1.at[own_rows, lo]), local(4, w_rq.at[:, col2], wg1.at[own_rows, hi])],
-        [local(5, w_rk.at[:, col2], wg2.at[own_rows, lo]), local(6, w_rv.at[:, col], wg2.at[own_rows, hi])],
-        [local(7, w_rg.at[:, col], wg3.at[own_rows])],
+        [local(3, w_rk.at[:, col2], wg1.at[own_rows, lo]), local(4, w_rv.at[:, col], wg1.at[own_rows, hi])],
+        [local(5, w_dq.at[:, col], wg2.at[own_rows])],
+        [local(6, w_rq.at[:, col2], wg3.at[own_rows, lo]), local(7, w_rg.at[:, col], wg3.at[own_rows, hi])],
     ]
     load_o = []
     for i in range(NX):
-        load_o.append(local(8 + 2 * i, w_ro.at[pl.ds(i * 128, 128)], wo.at[0, i, lo]))
-        load_o.append(local(9 + 2 * i, w_do.at[pl.ds(i * 128, 128)], wo.at[0, i, hi]))
+        src = (w_ro, w_do)[i // 2]
+        load_o.append(local(8 + i, src.at[pl.ds((i % 2) * 256, 256)], wo.at[0, i]))
 
     load_small = [
         local(16 + i, src, dst)
@@ -232,17 +232,17 @@
     pl.semaphore_wait(barrier, len(peers))
 
     phase("loads")
+    for copy in load_o:
+        copy.wait()
+    out_y.own()
     load_tok.wait()
     for ring in token_rings:
         ring.own()
     send(PART, tok.at[x, c], tok.at[x, c], partner)
     for copy in load_g[0]:
         copy.wait()
-    ring0[0].own()
-    for copy in load_o:
-        copy.wait()
-    out_y.own()
-    ring0[1].own()
+    for ring in ring0:
+        ring.own()
     for copy in load_small:
         copy.wait()
     for d in (1, 2, 3):
@@ -322,59 +322,56 @@
         kb[z, r, :] = rope(u, cosd[a, :], sind[a, :], 32).astype(BF16)
         vb[z, :, r] = proj[r, 128:256].T.astype(BF16)
 
-    phase("w0a")
-    ring0[0].near()
+    phase("oy")
+    out_y.near()
+    out_z[0].own()
     phase("tok_a")
     token_rings[0].near()
     part_send(1, order[1], 0, 64)
     part_send(2, order[2], 0, 64)
-    phase("oy")
-    out_y.near()
-    out_z[0].own()
-    phase("w0b")
-    ring0[1].near()
-    ring1.own()
+    phase("w0a")
+    ring0[0].near()
     phase("tok_b")
     token_rings[1].near()
     part_send(3, order[1], 64, 64)
     part_send(4, order[2], 64, 64)
+    phase("oy_far")
+    out_y.far()
+    out_z[1].own()
+    phase("oz_near")
+    out_z[0].near()
     phase("norm0")
     arrived(PART, tok.at[x, other])
     normalize(0)
-    phase("norm1")
-    part_arrived(1, order[1], 0, 64)
-    part_arrived(3, order[1], 64, 64)
-    normalize(1)
+    phase("w0b")
+    ring0[1].near()
+    ring1.own()
+    ring2.own()
     phase("tok_far_a")
     token_rings[0].far()
     part_send(5, order[3], 0, 64)
-    phase("oz_near")
-    out_z[0].near()
-    phase("norm2")
-    part_arrived(2, order[2], 0, 64)
-    part_arrived(4, order[2], 64, 64)
-    normalize(2)
+    phase("norm12")
+    for j in (1, 2):
+        part_arrived(j, order[j], 0, 64)
+        part_arrived(2 + j, order[j], 64, 64)
+        normalize(j)
     phase("tok_far_b")
     token_rings[1].far()
     part_send(6, order[3], 64, 64)
-    phase("oy_far")
-    out_y.far()
-    out_z[1].own()
-    phase("w0_far")
-    ring0[0].far()
-    ring0[1].far()
-    phase("project0")
-    project(0, 0, 384)
-    phase("kv_post")
-    for j in range(3):
-        keys_values(j)
+    phase("oz_far_near")
+    out_z[1].near()
     phase("norm3")
     part_arrived(5, order[3], 0, 64)
     part_arrived(6, order[3], 64, 64)
     normalize(3)
-    phase("project0b")
-    project(0, 384, 128)
-    keys_values(3)
+    phase("w0_far")
+    for ring in ring0:
+        ring.far()
+    phase("project0")
+    project(0)
+    phase("kv_post")
+    for j in range(4):
+        keys_values(j)
 
     zs = [(z + NZ + d) % NZ for d in range(-4, 5)]
 
@@ -394,6 +391,10 @@
         for way in (0, 1):
             kv_send(0, way, piece)
 
+    phase("levels")
+    phase("oz_near_far")
+    out_z[0].far()
+    out_x[0].own()
     phase("levels")
     for d in (1, 2, 3):
         arrived(DEC + d - 1, dec.at[xs[4 - d]])
@@ -410,82 +411,25 @@
         gcol[b * 128 : b * 128 + 128, :] = jnp.broadcast_to(row, (128, 128)).T
     dz[z] = jnp.broadcast_to(offset, (8, 128))
 
-    phase("oz_near_far")
-    out_z[0].far()
-    out_x[0].own()
-    out_z[1].near()
+    def kv_step(step, piece):
+        for way in (0, 1):
+            kv_arrived(step, way, piece)
+            if step < 2 or (step == 2 and piece == way):
+                kv_send(step + 1, way, piece)
+
     phase("w1")
     ring1.near()
-    ring2.own()
-    phase("oz_far_far")
-    out_z[1].far()
-    out_x[1].own()
-
-    def kv_step(step):
-        for piece in (0, 1):
-            for way in (0, 1):
-                kv_arrived(step, way, piece)
-                if step < 2 or (step == 2 and piece == way):
-                    kv_send(step + 1, way, piece)
-
+    phase("k0")
+    kv_step(0, 0)
+    phase("w2")
+    ring2.near()
+    ring3.own()
+    phase("v0")
+    kv_step(0, 1)
     phase("w1_far")
     ring1.far()
     phase("project1")
     project(1)
-    phase("q_post")
-    qgain = jnp.concatenate([qgain_in[x][0:1, :], qgain_in[x][1:2, :]], axis=1)
-    for i in range(NX):
-        r = slice(i * 128, i * 128 + 128)
-        a = block_rows(i)
-        u = map_norm(proj[r, 0:128], qgain)
-        u = rope(u, cosd[a, :], sind[a, :], 32).astype(BF16).astype(F32) * 0.125
-        u = u.T
-        s = slice((i % 2) * 128, (i % 2) * 128 + 128)
-        qbd[i // 2, :, s] = jnp.where(sub < 64, u, 0.0).astype(BF16)
-        qbd[2 + i // 2, :, s] = jnp.where(sub < 64, 0.0, u).astype(BF16)
-        rq[a, :] = rope(proj[r, 128:256], cosr[a, :], sinr[a, :], 64).astype(BF16)
-
-    m_run[...] = jnp.full((4, 1, 256), -jnp.inf, F32)
-    l_run[...] = jnp.zeros((4, 1, 256), F32)
-    acc[...] = jnp.zeros((4, 128, 256), F32)
-
-    def attend(*origins):
-        for q in range(4):
-            s = [jnp.dot(kb[o], qbd[q], preferred_element_type=F32) for o in origins]
-            before = m_run[q]
-            now = before
-            for part_s in s:
-                now = jnp.maximum(now, jnp.max(part_s, axis=0, keepdims=True))
-            shrink = jnp.exp(before - now)
-            m_run[q] = now
-            total = l_run[q] * shrink
-            value = acc[q] * shrink
-            for o, part_s in zip(origins, s):
-                e = jnp.exp(part_s - now)
-                total = total + jnp.sum(e, axis=0, keepdims=True)
-                value = value + jnp.dot(vb[o], e.astype(BF16), preferred_element_type=F32)
-            l_run[q] = total
-            acc[q] = value
-
-    phase("kv_step0")
-    kv_step(0)
-    phase("attend0")
-    attend(z)
-    phase("w2")
-    ring2.near()
-    ring3.own()
-    phase("attend1")
-    attend(at_z(-1), at_z(1))
-    phase("kv_step1")
-    kv_step(1)
-    phase("attend2")
-    attend(at_z(-2), at_z(2))
-    phase("ox_near")
-    out_x[0].near()
-    phase("w2_far")
-    ring2.far()
-    phase("project2")
-    project(2)
     phase("states")
     for i in range(NX):
         r = slice(i * 128, i * 128 + 128)
@@ -530,16 +474,91 @@
     st_send(0, 0)
     st_send(0, 1)
 
+    m_run[...] = jnp.full((4, 1, 256), -jnp.inf, F32)
+    l_run[...] = jnp.zeros((4, 1, 256), F32)
+    acc[...] = jnp.zeros((4, 128, 256), F32)
+
+    def attend(origins, tiles):
+        for q in tiles:
+            s = [jnp.dot(kb[o], qbd[q], preferred_element_type=F32) for o in origins]
+            before = m_run[q]
+            now = before
+            for part_s in s:
+                now = jnp.maximum(now, jnp.max(part_s, axis=0, keepdims=True))
+            shrink = jnp.exp(before - now)
+            m_run[q] = now
+            total = l_run[q] * shrink
+            value = acc[q] * shrink
+            for o, part_s in zip(origins, s):
+                e = jnp.exp(part_s - now)
+                total = total + jnp.sum(e, axis=0, keepdims=True)
+                value = value + jnp.dot(vb[o], e.astype(BF16), preferred_element_type=F32)
+            l_run[q] = total
+            acc[q] = value
+
+    phase("w2_far")
+    ring2.far()
+    phase("k1")
+    kv_step(1, 0)
+    phase("project2")
+    project(2)
+    phase("q_post")
+    query_order = [3, 1, 2, 0]
+    qgain = jnp.concatenate([qgain_in[x][0:1, :], qgain_in[x][1:2, :]], axis=1)
+    for p, i in enumerate(query_order):
+        r = slice(i * 128, i * 128 + 128)
+        a = block_rows(i)
+        u = map_norm(proj[r, 0:128], qgain)
+        u = rope(u, cosd[a, :], sind[a, :], 32).astype(BF16).astype(F32) * 0.125
+        u = u.T
+        s = slice((p % 2) * 128, (p % 2) * 128 + 128)
+        qbd[p // 2, :, s] = jnp.where(sub < 64, u, 0.0).astype(BF16)
+        qbd[2 + p // 2, :, s] = jnp.where(sub < 64, 0.0, u).astype(BF16)
+
+    phase("v1")
+    kv_step(1, 1)
+    phase("attend0a")
+    attend((z,), (0, 1))
+    phase("oz_far_far")
+    out_z[1].far()
+    out_x[1].own()
+    phase("st_step0")
+    st_step(0)
+    phase("attend0b")
+    attend((z,), (2, 3))
+    phase("ox_near")
+    out_x[0].near()
+    phase("attend1a")
+    attend((at_z(-1), at_z(1)), (0, 1))
+    phase("k2")
+    kv_step(2, 0)
+    phase("attend1b")
+    attend((at_z(-1), at_z(1)), (2, 3))
     phase("w3")
     ring3.near()
-    phase("kv_step2")
-    kv_step(2)
-    phase("attend3")
-    attend(at_z(-3), at_z(3))
-    phase("st_step0")
-    st_step(0)
+    phase("attend2a")
+    attend((at_z(-2), at_z(2)), (0, 1))
+    phase("v2")
+    kv_step(2, 1)
+    phase("attend2b")
+    attend((at_z(-2), at_z(2)), (2, 3))
+    phase("st_step1")
+    st_step(1)
     phase("ox_far")
     out_x[1].near()
+    phase("w3_far")
+    ring3.far()
+    phase("project3")
+    project(3)
+    for i in range(NX):
+        r = slice(i * 128, i * 128 + 128)
+        a = block_rows(i)
+        rq[a, :] = rope(proj[r, 0:128], cosr[a, :], sinr[a, :], 64).astype(BF16)
+        gate[i] = proj[r, 128:256].astype(BF16)
+    for d, j in ((1, 2), (2, 3), (3, 1)):
+        send(GT + d - 1, gate.at[j], gt.at[x], along_x(xs[d]))
+    gt[x] = gate[0]
+
     phase("intra")
     for i in range(NX):
         r = slice(i * 128, i * 128 + 128)
@@ -548,41 +567,35 @@
         w = (s * jnp.exp(-jnp.abs(level - grow[...]))).astype(BF16)
         mix[i] = jnp.dot(w, rv[...], preferred_element_type=F32)
 
-    phase("st_step1")
-    st_step(1)
-    phase("w3_far")
-    ring3.far()
-    phase("gate")
-    project(3)
-    for i in range(NX):
-        gate[i] = proj[i * 128 : i * 128 + 128, 0:128].astype(BF16)
-    for d, j in ((1, 2), (2, 3), (3, 1)):
-        send(GT + d - 1, gate.at[j], gt.at[x], along_x(xs[d]))
-    gt[x] = gate[0]
-
+    phase("attend3a")
+    attend((at_z(-3), at_z(3)), (0, 2))
     phase("st_step2")
     st_step(2)
+    phase("attend3b")
+    attend((at_z(-3), at_z(3)), (1, 3))
     phase("kv_last")
     kv_arrived(3, 0, 0)
     kv_arrived(3, 1, 1)
-    phase("attend4")
-    attend(at_z(4))
-    phase("diff_out")
 
     lane4 = lax.broadcasted_iota(jnp.int32, (1, 4), 1)
     lam = jnp.sum(jnp.where(lane4 == x, lam_in[...], 0.0), axis=-1, keepdims=True)
     dgain = dgain_in[pl.ds(x, 1), :]
-    for t in range(2):
+
+    def differ_out(t):
         first = acc[t] / l_run[t]
         second = acc[2 + t] / l_run[2 + t]
         both = first - lam * second
         both = both * lax.rsqrt(jnp.mean(both * both, axis=0, keepdims=True) + EPS)
         for h in range(2):
-            feat[2 * t + h] = (both[:, h * 128 : h * 128 + 128].T * dgain).astype(BF16)
-    for d, j in ((1, 2), (2, 3), (3, 1)):
-        send(DF + d - 1, feat.at[j], df.at[x], along_x(xs[d]))
-    df[x] = feat[0]
-
+            j = query_order[2 * t + h]
+            feat[j] = (both[:, h * 128 : h * 128 + 128].T * dgain).astype(BF16)
+
+    phase("attend4a")
+    attend((at_z(4),), (0, 2))
+    phase("differ_out_a")
+    differ_out(0)
+    send(DF + 1, feat.at[3], df.at[x], along_x(xs[2]))
+    send(DF + 2, feat.at[1], df.at[x], along_x(xs[3]))
     phase("st_step3")
     st_step(3)
     phase("carried")
@@ -607,36 +620,50 @@
             [(query * jnp.exp(level)).astype(BF16), (query * jnp.exp(end - level)).astype(BF16)],
             axis=1,
         )
-        mix[i] = mix[i] + jnp.dot(q2, states, preferred_element_type=F32)
-    for d in (1, 2, 3):
-        send(RM + d - 1, mix.at[xs[d]], rm.at[x], along_x(xs[d]))
-    rm[x] = mix[x]
-
-    phase("o2_far")
+        total = mix[i] + jnp.dot(q2, states, preferred_element_type=F32)
+        mixed[i] = total.astype(BF16)
+    send(RM + 1, mixed.at[xs[2]], rm.at[x], along_x(xs[2]))
+    send(RM, mixed.at[xs[1]], rm.at[x], along_x(xs[1]))
+    send(RM + 2, mixed.at[xs[3]], rm.at[x], along_x(xs[3]))
+    rm[x] = mixed[x]
+    phase("attend4b")
+    attend((at_z(4),), (1, 3))
+    phase("differ_out_b")
+    differ_out(1)
+    send(DF, feat.at[2], df.at[x], along_x(xs[1]))
+    df[x] = feat[0]
+
+    phase("ox_far_far")
     for ring in out_x:
         ring.far()
-    phase("home_wait")
+    phase("home_wait_r")
     for d in (1, 2, 3):
         arrived(GT + d - 1, gt.at[xs[4 - d]])
-        arrived(DF + d - 1, df.at[xs[4 - d]])
         arrived(RM + d - 1, rm.at[xs[4 - d]])
-    phase("home")
+    phase("home_r")
     for h in range(2):
-        a, b = rm[2 * h], rm[2 * h + 1]
+        a, b = rm[2 * h].astype(F32), rm[2 * h + 1].astype(F32)
         total = jnp.sum(a * a, axis=-1, keepdims=True) + jnp.sum(b * b, axis=-1, keepdims=True)
         scale = lax.rsqrt(total / 256 + EPS)
         for k, m in ((2 * h, a), (2 * h + 1, b)):
             g = gt[k].astype(F32)
             value = (g * jax.nn.sigmoid(g)) * (m * scale * rgain_in[k : k + 1, :])
-            fall[:, k * 256 : k * 256 + 128] = value.astype(BF16)
-            fall[:, k * 256 + 128 : k * 256 + 256] = df[k]
-
+            fall[:, k * 128 : k * 128 + 128] = value.astype(BF16)
+    for k in range(NY):
+        w = wo[k].reshape(1024, 512)[0:512]
+        total_out[k] = jnp.dot(fall[:, 0:512], w, preferred_element_type=F32)
+    phase("home_wait_d")
+    for d in (1, 2, 3):
+        arrived(DF + d - 1, df.at[xs[4 - d]])
+    for k in range(NX):
+        fall[:, 512 + k * 128 : 640 + k * 128] = df[k]
     phase("out_dot")
     mine = pl.ds(pl.multiple_of(c * 64, 64), 64)
     theirs = pl.ds(pl.multiple_of(other * 64, 64), 64)
     for k in range(NY):
-        w = wo[k].reshape(1024, 512)
-        part[k] = jnp.dot(fall[...], w, preferred_element_type=F32).astype(BF16)
+        w = wo[k].reshape(1024, 512)[512:1024]
+        total = total_out[k] + jnp.dot(fall[:, 512:1024], w, preferred_element_type=F32)
+        part[k] = total.astype(BF16)
         send(OUT + k, part.at[k, theirs], pin.at[k], partner)
     phase("out_wait")
     for k in range(NY):
@@ -667,7 +694,7 @@
             V((4, 128), F32), V((4, 128), F32), V((1, D), F32), V((4, 64, 128), F32),
             V((NX, 2, 128, 1024), BF16),
             V((BLOCK, D), BF16),
-            V((D, 256), BF16), V((D, 256), BF16), V((D, 256), BF16), V((D, 128), BF16),
+            V((D, 256), BF16), V((D, 256), BF16), V((D, 128), BF16), V((D, 256), BF16),
             V((NY, NX, 256, 512), BF16),
             V((NX, 2, 128), F32),
             V((NZ, BLOCK, 128), BF16),
@@ -675,16 +702,17 @@
             V((NZ, 2, 128, 128), BF16),
             V((NZ, 8, 128), F32),
             V((BLOCK, 128), F32), V((BLOCK, 128), F32), V((BLOCK, 128), F32), V((BLOCK, 128), F32),
-            V((BLOCK, 256), F32),
+            V((BLOCK, 256), F32), V((BLOCK, 128), F32),
             V((4, 128, 256), BF16),
             V((4, 1, 256), F32), V((4, 1, 256), F32), V((4, 128, 256), F32),
             V((BLOCK, 128), BF16), V((BLOCK, 128), BF16), V((BLOCK, 128), BF16),
             V((1, BLOCK), F32), V((BLOCK, 128), F32),
             V((NX, 128, 128), F32),
             V((NX, 128, 128), BF16), V((NX, 128, 128), BF16),
-            V((NX, 128, 128), BF16), V((NX, 128, 128), BF16), V((NX, 128, 128), F32),
+            V((NX, 128, 128), BF16), V((NX, 128, 128), BF16), V((NX, 128, 128), BF16),
             V((128, 1024), BF16),
             V((NY, 128, 512), BF16), V((NY, 64, 512), BF16),
+            V((NX, 128, 128), BF16), V((NY, 128, 512), F32),
             pltpu.SemaphoreType.DMA((COPIES,)),
             pltpu.SemaphoreType.DMA((COPIES,)),
             pltpu.SemaphoreType.DMA((LOCALS,)),

time: 75.7 us -> 69 us (0.911)
  Pallas kernels: 73.9 us -> 67.2 us
    pallas_call x1, Pallas kernels: 73.9 us -> 67.2 us  [body(): pl.pallas_call(kernel, out_shape=jax.ShapeDtypeStruct((1, 64, D), BF16),...]
where the time goes in v3:
time: 69 us; the launch traced here: 68.9 us
  Pallas kernels  67.2 us (97%)
  local copies, waits for them, and re-layouts  1.67 us (2%)
    pallas_call x1, Pallas kernels, body(): pl.pallas_call(kernel, out_shape=jax.ShapeDtypeStruct((1, 64, D), BF16),...  67.2 us
    unnamed x1, local copies, waits for them, and re-layouts  1.67 us

profile of v3, /device:TPU:1, one launch (start us, length us, event | category | flops | bytes accessed | tf_op | source)
XLA Modules:
  0.0 68.9 jit_solution(11278916616069414938)
XLA Ops:
  0.0 67.2 %shard_map.172 = bf16[1,64,2048]{2,1,0:T(8,128)(2,1)} custom-call(bf16[1,128,1024]{2,1,0:T(8,128)(2,1)} %tok_in.1, bf16[512,256]{1,0:T(8,128)(2,1)} %w_rq.1, bf16[512,256]{1,0:T(8,128)(2,1)} %w_rk.1, bf16[512,512]{1,0:T(8,128)(2,1)} %w_rv.1, bf16[512,512]{1,0:T(8,128)(2,1)} %w_rg.1, bf16[512,512]{1,0:T(8,128)(2,1)} %w_dq.1, bf16[512,512]{1,0:T(8,128)(2,1)} %w_dk.1, ...), custom_call_target="tpu_custom_call" | custom-call | tf_op jit(solution)/shard_map/pallas_call | solution.py:687
  67.2 1.7 %copy.20 = bf16[1,64,2048]{2,1,0:T(8,128)(2,1)} copy(bf16[1,64,2048]{2,1,0:T(8,128)(2,1)} %shard_map.172) | data formatting | bytes 524288

commit v4 on v3

--- a/solution.py
+++ b/solution.py
@@ -36,7 +36,8 @@
 RM = 97
 OUT = 100
 COPIES = 104
-LOCALS = 24
+SENDS = 50
+LOCALS = 20
 
 
 def rope_tables():
@@ -68,7 +69,7 @@
     dec_hbm, lam_hbm, qgain_hbm, kgain_hbm, rgain_hbm, dgain_hbm, ngain_hbm, tab_hbm,
     out,
     dec_in, lam_in, qgain_in, kgain_in, rgain_in, dgain_in, gain_in, tab, tok, xn, wg0, wg1, wg2, wg3, wo, dec, kb, vb, st, dz, cosd, sind, cosr, sinr, proj, proj2, qbd,
-    m_run, l_run, acc, rq, rk, rv, grow, gcol, mix, gate, feat, df, gt, rm, fall, part, pin, mixed, total_out,
+    m_run, l_run, acc, rq, rk, rv, grow, gcol, mix, gate, feat, df, gt, rm, fall, part, mixed, total_out,
     ssem, rsem, lsem,
 ):
     phase = Phases()
@@ -92,39 +93,43 @@
     ys = [y, (y + 1) % NY, (y + 2) % NY, (y + 3) % NY]
     zr, zl = (z + 1) % NZ, (z + NZ - 1) % NZ
 
-    def remote(i, src, dst, device):
-        return pltpu.make_async_remote_copy(
-            src_ref=src, dst_ref=dst, send_sem=ssem.at[i], recv_sem=rsem.at[i],
+    sent = []
+    rings_sent = {}
+
+    def send(i, src, dst, device, ring=None):
+        n = len(sent) if ring is None else rings_sent.setdefault(id(ring), (len(sent), ring))[0]
+        copy = pltpu.make_async_remote_copy(
+            src_ref=src, dst_ref=dst, send_sem=ssem.at[n], recv_sem=rsem.at[i],
             device_id=device, device_id_type=MESH,
         )
-
-    sent = []
-
-    def send(i, src, dst, device):
-        copy = remote(i, src, dst, device)
         copy.start()
-        sent.append(copy)
+        if n == len(sent):
+            sent.append(copy if ring is None else None)
 
     def arrived(i, ref):
-        remote(i, ref, ref, partner).wait_recv()
+        pltpu.make_async_remote_copy(
+            src_ref=ref, dst_ref=ref, send_sem=ssem.at[0], recv_sem=rsem.at[i],
+            device_id=partner, device_id_type=MESH,
+        ).wait_recv()
 
     class Ring4:
-        def __init__(self, base, right, left, own, to_right, to_left, half, onward, far):
+        def __init__(self, base, right, left, own, to_right, to_left, half, onward, far, three):
             self.base, self.right, self.left = base, right, left
             self.src, self.to_right, self.to_left, self.half = own, to_right, to_left, half
             self.onward, self.far_half = onward, far
+            self.three = three
 
         def own(self):
-            send(self.base, self.src, self.to_right, self.right)
-            send(self.base + 1, self.src, self.to_left, self.left)
+            send(self.base, self.src, self.to_right, self.right, self.three)
+            send(self.base + 1, self.src, self.to_left, self.left, self.three)
 
         def wait(self):
             arrived(self.base, self.half[2])
             arrived(self.base + 1, self.half[3])
 
         def forward(self):
-            send(self.base + 2, self.half[0], self.onward[0], self.right)
-            send(self.base + 3, self.half[1], self.onward[1], self.left)
+            send(self.base + 2, self.half[0], self.onward[0], self.right, self.three)
+            send(self.base + 3, self.half[1], self.onward[1], self.left, self.three)
 
         def near(self):
             self.wait()
@@ -134,34 +139,71 @@
             arrived(self.base + 2, self.far_half[0])
             arrived(self.base + 3, self.far_half[1])
 
-    def ring_at(base, at, sides, full, half):
+    def ring_at(base, at, sides, full, half, three):
         return Ring4(
             base, sides[0], sides[1], full(at[0]), full(at[0]), full(at[0]),
             (half(at[3], 0), half(at[1], 1), full(at[3]), full(at[1])),
-            (half(at[3], 0), half(at[1], 1)), (half(at[2], 0), half(at[2], 1)),
+            (half(at[3], 0), half(at[1], 1)), (half(at[2], 0), half(at[2], 1)), three,
         )
 
     wgs = (wg0, wg1, wg2, wg3)
     def rows_of(start, size):
         return pl.ds(pl.multiple_of(start, size & -size), size)
 
-    token_rings = [
-        ring_at(
-            TOK + 4 * piece, xs, (along_x(xs[1]), along_x(xs[3])),
-            lambda i, p=piece: tok.at[i, c, pl.ds(p * 64, 64)],
-            lambda i, h, p=piece: tok.at[i, c, pl.ds(p * 64 + h * 32, 32)],
-        )
-        for piece in (0, 1)
-    ]
+    def token_half(i, h):
+        return tok.at[i, c, pl.ds(h * 64, 64)]
+
+    six = tok.at[pl.ds(0, 3), 0]
+
+    def token_send(n, i, h, to):
+        send(TOK + n, token_half(i, h), token_half(i, h), along_x(xs[to]), six)
+
+    def tokens_own():
+        for n, h, to in ((0, 0, 1), (1, 1, 3), (2, 1, 1), (3, 0, 3)):
+            token_send(n, xs[0], h, to)
+
+    def tokens_first():
+        arrived(TOK, token_half(xs[3], 0))
+        token_send(4, xs[3], 0, 1)
+        arrived(TOK + 1, token_half(xs[1], 1))
+        token_send(5, xs[1], 1, 3)
+
+    def tokens_second():
+        arrived(TOK + 2, token_half(xs[3], 1))
+        arrived(TOK + 3, token_half(xs[1], 0))
 
     def weight_ring(base, ref, start, size):
         return ring_at(
             base, ys, (along_y(ys[1]), along_y(ys[3])),
             lambda i: ref.at[rows_of(i * 512 + start, size)],
             lambda i, h: ref.at[rows_of(i * 512 + start + h * (size // 2), size // 2)],
+            ref.at[pl.ds(start, 3 * size)],
         )
 
-    ring0 = [weight_ring(W0 + 4 * piece, wg0, piece * 256, 256) for piece in (0, 1)]
+    def weight_half(i, h):
+        return wg0.at[rows_of(i * 512 + h * 256, 256)]
+
+    three_blocks = wg0.at[pl.ds(0, 1536)]
+
+    def weight_send(n, i, h, to):
+        send(W0 + n, weight_half(i, h), weight_half(i, h), along_y(ys[to]), three_blocks)
+
+    def weights_own():
+        for n, h, to in ((0, 0, 1), (1, 1, 3), (2, 1, 1), (3, 0, 3)):
+            weight_send(n, ys[0], h, to)
+
+    def weights_first():
+        arrived(W0, weight_half(ys[3], 0))
+        weight_send(4, ys[3], 0, 1)
+        arrived(W0 + 1, weight_half(ys[1], 1))
+        weight_send(5, ys[1], 1, 3)
+
+    def weights_rest():
+        arrived(W0 + 2, weight_half(ys[3], 1))
+        arrived(W0 + 3, weight_half(ys[1], 0))
+        arrived(W0 + 4, weight_half(ys[2], 0))
+        arrived(W0 + 5, weight_half(ys[2], 1))
+
     ring1 = weight_ring(W1, wg1, 0, 512)
     ring2 = weight_ring(W2, wg2, 0, 512)
     ring3 = weight_ring(W3, wg3, 0, 512)
@@ -178,6 +220,7 @@
         OY, along_y(ys[1]), along_y(ys[3]), slice_of(0, zc), slice_of(2, zc), slice_of(1, zc),
         (slice_of(2, zc, 0), slice_of(1, zc, 1), slice_of(2, zc), slice_of(1, zc)),
         (slice_of(3, zc, 0), slice_of(3, zc, 1)), (slice_of(3, zc, 0), slice_of(3, zc, 1)),
+        wo.at[0, 0, pl.ds(0, 192)],
     )
 
     near, far = pl.ds(1, 2), 3
@@ -185,12 +228,13 @@
     out_x = []
     for k, slot in enumerate((near, far)):
         piece = functools.partial(slice_of, slot)
-        out_z.append(ring_at(OZ + 4 * k, zcs, (along_z(zr), along_z(zl)), piece, piece))
+        out_z.append(ring_at(OZ + 4 * k, zcs, (along_z(zr), along_z(zl)), piece, piece, wo.at[slot, 0, pl.ds(0, 192)]))
         out_x.append(
             ring_at(
                 OX + 4 * k, xs, (along_x(xs[1]), along_x(xs[3])),
                 lambda i, s=slot: wo.at[s, i],
                 lambda i, h, s=slot: wo.at[s, i, pl.ds(h * 128, 128)],
+                wo.at[slot, pl.ds(0, 3)],
             )
         )
 
@@ -216,7 +260,7 @@
         load_o.append(local(8 + i, src.at[pl.ds((i % 2) * 256, 256)], wo.at[0, i]))
 
     load_small = [
-        local(16 + i, src, dst)
+        local(12 + i, src, dst)
         for i, (src, dst) in enumerate((
             (dec_hbm, dec_in), (lam_hbm, lam_in), (qgain_hbm, qgain_in), (kgain_hbm, kgain_in),
             (rgain_hbm, rgain_in), (dgain_hbm, dgain_in), (ngain_hbm, gain_in), (tab_hbm, tab),
@@ -232,22 +276,20 @@
     pl.semaphore_wait(barrier, len(peers))
 
     phase("loads")
-    for copy in load_o:
-        copy.wait()
-    out_y.own()
-    load_tok.wait()
-    for ring in token_rings:
-        ring.own()
-    send(PART, tok.at[x, c], tok.at[x, c], partner)
-    for copy in load_g[0]:
-        copy.wait()
-    for ring in ring0:
-        ring.own()
     for copy in load_small:
         copy.wait()
     for d in (1, 2, 3):
         send(DEC + d - 1, dec_in, dec.at[x], along_x(xs[d]))
     dec[x] = dec_in[...]
+    for copy in load_o:
+        copy.wait()
+    out_y.own()
+    load_tok.wait()
+    tokens_own()
+    send(PART, tok.at[x, c], tok.at[x, c], partner)
+    for copy in load_g[0]:
+        copy.wait()
+    weights_own()
     for group in load_g[1:]:
         for copy in group:
             copy.wait()
@@ -325,76 +367,6 @@
     phase("oy")
     out_y.near()
     out_z[0].own()
-    phase("tok_a")
-    token_rings[0].near()
-    part_send(1, order[1], 0, 64)
-    part_send(2, order[2], 0, 64)
-    phase("w0a")
-    ring0[0].near()
-    phase("tok_b")
-    token_rings[1].near()
-    part_send(3, order[1], 64, 64)
-    part_send(4, order[2], 64, 64)
-    phase("oy_far")
-    out_y.far()
-    out_z[1].own()
-    phase("oz_near")
-    out_z[0].near()
-    phase("norm0")
-    arrived(PART, tok.at[x, other])
-    normalize(0)
-    phase("w0b")
-    ring0[1].near()
-    ring1.own()
-    ring2.own()
-    phase("tok_far_a")
-    token_rings[0].far()
-    part_send(5, order[3], 0, 64)
-    phase("norm12")
-    for j in (1, 2):
-        part_arrived(j, order[j], 0, 64)
-        part_arrived(2 + j, order[j], 64, 64)
-        normalize(j)
-    phase("tok_far_b")
-    token_rings[1].far()
-    part_send(6, order[3], 64, 64)
-    phase("oz_far_near")
-    out_z[1].near()
-    phase("norm3")
-    part_arrived(5, order[3], 0, 64)
-    part_arrived(6, order[3], 64, 64)
-    normalize(3)
-    phase("w0_far")
-    for ring in ring0:
-        ring.far()
-    phase("project0")
-    project(0)
-    phase("kv_post")
-    for j in range(4):
-        keys_values(j)
-
-    zs = [(z + NZ + d) % NZ for d in range(-4, 5)]
-
-    def at_z(d):
-        return zs[d + 4]
-
-    def kv_send(step, way, piece):
-        origin = at_z(-step if way == 0 else step)
-        ref = (kb, vb)[piece].at[origin]
-        send(KV + 4 * step + 2 * way + piece, ref, ref, along_z(zr if way == 0 else zl))
-
-    def kv_arrived(step, way, piece):
-        origin = at_z(-(step + 1) if way == 0 else step + 1)
-        arrived(KV + 4 * step + 2 * way + piece, (kb, vb)[piece].at[origin])
-
-    for piece in (0, 1):
-        for way in (0, 1):
-            kv_send(0, way, piece)
-
-    phase("levels")
-    phase("oz_near_far")
-    out_z[0].far()
-    out_x[0].own()
     phase("levels")
     for d in (1, 2, 3):
         arrived(DEC + d - 1, dec.at[xs[4 - d]])
@@ -417,6 +389,74 @@
             if step < 2 or (step == 2 and piece == way):
                 kv_send(step + 1, way, piece)
 
+    phase("tok_a")
+    tokens_first()
+    part_send(1, order[1], 0, 64)
+    part_send(2, order[2], 64, 64)
+    phase("w0a")
+    weights_first()
+    ring1.own()
+    ring2.own()
+    phase("tok_b")
+    tokens_second()
+    part_send(3, order[1], 64, 64)
+    part_send(4, order[2], 0, 64)
+    phase("norm0")
+    arrived(PART, tok.at[x, other])
+    normalize(0)
+    phase("oz_near")
+    out_z[0].near()
+    phase("tok_far_a")
+    arrived(TOK + 4, token_half(xs[2], 0))
+    part_send(5, order[3], 0, 64)
+    phase("norm12")
+    for j in (1, 2):
+        part_arrived(j, order[j], (j - 1) * 64, 64)
+        part_arrived(2 + j, order[j], (2 - j) * 64, 64)
+        normalize(j)
+    phase("oy_far")
+    out_y.far()
+    out_z[1].own()
+    phase("tok_far_b")
+    arrived(TOK + 5, token_half(xs[2], 1))
+    part_send(6, order[3], 64, 64)
+    phase("norm3")
+    part_arrived(5, order[3], 0, 64)
+    part_arrived(6, order[3], 64, 64)
+    normalize(3)
+    phase("w0_far")
+    weights_rest()
+    phase("project0")
+    project(0)
+    phase("kv_post")
+    for j in range(4):
+        keys_values(j)
+
+    zs = [(z + NZ + d) % NZ for d in range(-4, 5)]
+
+    def at_z(d):
+        return zs[d + 4]
+
+    kv_rings = [kb.at[pl.ds(0, 7)], vb.at[pl.ds(0, 7)]]
+
+    def kv_send(step, way, piece):
+        origin = at_z(-step if way == 0 else step)
+        ref = (kb, vb)[piece].at[origin]
+        send(KV + 4 * step + 2 * way + piece, ref, ref, along_z(zr if way == 0 else zl), kv_rings[piece])
+
+    def kv_arrived(step, way, piece):
+        origin = at_z(-(step + 1) if way == 0 else step + 1)
+        arrived(KV + 4 * step + 2 * way + piece, (kb, vb)[piece].at[origin])
+
+    for piece in (0, 1):
+        for way in (0, 1):
+            kv_send(0, way, piece)
+
+    phase("oz_near_far")
+    out_z[0].far()
+    out_x[0].own()
+    phase("oz_far_near")
+    out_z[1].near()
     phase("w1")
     ring1.near()
     phase("k0")
@@ -660,19 +700,29 @@
     phase("out_dot")
     mine = pl.ds(pl.multiple_of(c * 64, 64), 64)
     theirs = pl.ds(pl.multiple_of(other * 64, 64), 64)
+    own_copies = []
     for k in range(NY):
         w = wo[k].reshape(1024, 512)[512:1024]
         total = total_out[k] + jnp.dot(fall[:, 512:1024], w, preferred_element_type=F32)
         part[k] = total.astype(BF16)
-        send(OUT + k, part.at[k, theirs], pin.at[k], partner)
+        columns = rows_of(ys[(0, 1, 3, 2)[k]] * 512, 512)
+        send(OUT + k, part.at[k, theirs], out.at[1, :, columns], partner)
+        own_copies.append(local(8 + k, part.at[k, mine], out.at[0, :, columns]))
     phase("out_wait")
     for k in range(NY):
-        arrived(OUT + k, pin.at[k])
-        value = part[k, mine, :].astype(F32) + pin[k].astype(F32)
-        out[0, :, rows_of(ys[(0, 1, 3, 2)[k]] * 512, 512)] = value.astype(BF16)
+        arrived(OUT + k, out.at[1, :, rows_of(ys[(0, 1, 3, 2)[k]] * 512, 512)])
+    for copy in own_copies:
+        copy.wait()
     phase("drain")
     for copy in sent:
-        copy.wait_send()
+        if copy is not None:
+            copy.wait_send()
+    for n, ref in rings_sent.values():
+        pltpu.make_async_remote_copy(
+            src_ref=ref, dst_ref=ref, send_sem=ssem.at[n], recv_sem=rsem.at[0],
+            device_id=partner, device_id_type=MESH,
+        ).wait_send()
+    assert len(sent) == SENDS, len(sent)
     phase(None)
 
 
@@ -682,13 +732,12 @@
     differ_gain, retain_out, differ_out,
 ):
     hbm = pl.BlockSpec(memory_space=pltpu.HBM)
-    vmem = pl.BlockSpec(memory_space=pltpu.VMEM)
     V = pltpu.VMEM
-    return pl.pallas_call(
+    parts = pl.pallas_call(
         kernel,
-        out_shape=jax.ShapeDtypeStruct((1, 64, D), BF16),
+        out_shape=jax.ShapeDtypeStruct((2, 64, D), BF16),
         in_specs=[hbm] * 18,
-        out_specs=vmem,
+        out_specs=hbm,
         scratch_shapes=[
             V((2, 128), F32), V((1, 4), F32), V((4, 2, 64), F32), V((4, 2, 64), F32),
             V((4, 128), F32), V((4, 128), F32), V((1, D), F32), V((4, 64, 128), F32),
@@ -711,9 +760,9 @@
             V((NX, 128, 128), BF16), V((NX, 128, 128), BF16),
             V((NX, 128, 128), BF16), V((NX, 128, 128), BF16), V((NX, 128, 128), BF16),
             V((128, 1024), BF16),
-            V((NY, 128, 512), BF16), V((NY, 64, 512), BF16),
+            V((NY, 128, 512), BF16),
             V((NX, 128, 128), BF16), V((NY, 128, 512), F32),
-            pltpu.SemaphoreType.DMA((COPIES,)),
+            pltpu.SemaphoreType.DMA((SENDS,)),
             pltpu.SemaphoreType.DMA((COPIES,)),
             pltpu.SemaphoreType.DMA((LOCALS,)),
         ],
@@ -726,6 +775,7 @@
         key_gain, retain_gain.reshape(4, 128), differ_gain.reshape(4, 128), norm_gain.reshape(1, D),
         jnp.asarray(rope_tables()),
     )
+    return (parts[0:1].astype(F32) + parts[1:2].astype(F32)).astype(BF16)
 
 
 def solution(mesh):

time: 69 us -> 66.4 us (0.962)
  Pallas kernels: 67.2 us -> 64.5 us
  other arithmetic: 0 us -> 1.8 us
  local copies, waits for them, and re-layouts: 1.67 us -> 0 us
    pallas_call x1, Pallas kernels: 67.2 us -> 64.5 us  [body(): pl.pallas_call(kernel, out_shape=jax.ShapeDtypeStruct((2, 64, D), BF16),...]
    convert_element_type x0 -> x1, other arithmetic: none -> 1.8 us  [body(): return (parts[0:1].astype(F32) + parts[1:2].astype(F32)).astype(BF16)]
    unnamed x1 -> x0, local copies, waits for them, and re-layouts: 1.67 us -> none
where the time goes in v4:
time: 66.4 us; the launch traced here: 66.3 us
  Pallas kernels  64.5 us (97%)
  other arithmetic  1.8 us (3%)
    pallas_call x1, Pallas kernels, body(): pl.pallas_call(kernel, out_shape=jax.ShapeDtypeStruct((2, 64, D), BF16),...  64.5 us
    convert_element_type x1, other arithmetic, body(): return (parts[0:1].astype(F32) + parts[1:2].astype(F32)).astype(BF16)  1.8 us

profile of v4, /device:TPU:1, one launch (start us, length us, event | category | flops | bytes accessed | tf_op | source)
XLA Modules:
  0.0 66.3 jit_solution(10482178124743440607)
XLA Ops:
  0.0 64.5 %shard_map.172 = bf16[2,64,2048]{2,1,0:T(8,128)(2,1)} custom-call(bf16[1,128,1024]{2,1,0:T(8,128)(2,1)} %tok_in.1, bf16[512,256]{1,0:T(8,128)(2,1)} %w_rq.1, bf16[512,256]{1,0:T(8,128)(2,1)} %w_rk.1, bf16[512,512]{1,0:T(8,128)(2,1)} %w_rv.1, bf16[512,512]{1,0:T(8,128)(2,1)} %w_rg.1, bf16[512,512]{1,0:T(8,128)(2,1)} %w_dq.1, bf16[512,512]{1,0:T(8,128)(2,1)} %w_dk.1, ...), custom_call_target="tpu_custom_call" | custom-call | tf_op jit(solution)/shard_map/pallas_call | solution.py:736
  64.5 1.8 %add_convert_fusion = bf16[1,64,2048]{2,1,0:T(8,128)(2,1)} fusion(bf16[2,64,2048]{2,1,0:T(8,128)(2,1)} %shard_map.172), kind=kLoop, calls=%fused_computation | loop fusion | flops 524288 | bytes 786432 | tf_op jit(solution)/shard_map/convert_element_type | solution.py:778

commit v5 on v4

--- a/solution.py
+++ b/solution.py
@@ -555,17 +555,17 @@
         qbd[p // 2, :, s] = jnp.where(sub < 64, u, 0.0).astype(BF16)
         qbd[2 + p // 2, :, s] = jnp.where(sub < 64, 0.0, u).astype(BF16)
 
+    phase("attend0a")
+    attend((z,), (0, 1))
     phase("v1")
     kv_step(1, 1)
-    phase("attend0a")
-    attend((z,), (0, 1))
     phase("oz_far_far")
     out_z[1].far()
     out_x[1].own()
+    phase("attend0b")
+    attend((z,), (2, 3))
     phase("st_step0")
     st_step(0)
-    phase("attend0b")
-    attend((z,), (2, 3))
     phase("ox_near")
     out_x[0].near()
     phase("attend1a")
@@ -586,6 +586,10 @@
     st_step(1)
     phase("ox_far")
     out_x[1].near()
+    phase("attend3a")
+    attend((at_z(-3), at_z(3)), (0, 2))
+    phase("st_step2")
+    st_step(2)
     phase("w3_far")
     ring3.far()
     phase("project3")
@@ -607,10 +611,6 @@
         w = (s * jnp.exp(-jnp.abs(level - grow[...]))).astype(BF16)
         mix[i] = jnp.dot(w, rv[...], preferred_element_type=F32)
 
-    phase("attend3a")
-    attend((at_z(-3), at_z(3)), (0, 2))
-    phase("st_step2")
-    st_step(2)
     phase("attend3b")
     attend((at_z(-3), at_z(3)), (1, 3))
     phase("kv_last")

time: 66.4 us -> 66.4 us (level)
  no operation moved by 1% of the time
where the time goes in v5:
time: 66.4 us; the launch traced here: 66.3 us
  Pallas kernels  64.5 us (97%)
  other arithmetic  1.8 us (3%)
    pallas_call x1, Pallas kernels, body(): pl.pallas_call(kernel, out_shape=jax.ShapeDtypeStruct((2, 64, D), BF16),...  64.5 us
    convert_element_type x1, other arithmetic, body(): return (parts[0:1].astype(F32) + parts[1:2].astype(F32)).astype(BF16)  1.8 us

profile of v5, /device:TPU:1, one launch (start us, length us, event | category | flops | bytes accessed | tf_op | source)
XLA Modules:
  0.0 66.3 jit_solution(5900303501645900432)
XLA Ops:
  0.0 64.5 %shard_map.172 = bf16[2,64,2048]{2,1,0:T(8,128)(2,1)} custom-call(bf16[1,128,1024]{2,1,0:T(8,128)(2,1)} %tok_in.1, bf16[512,256]{1,0:T(8,128)(2,1)} %w_rq.1, bf16[512,256]{1,0:T(8,128)(2,1)} %w_rk.1, bf16[512,512]{1,0:T(8,128)(2,1)} %w_rv.1, bf16[512,512]{1,0:T(8,128)(2,1)} %w_rg.1, bf16[512,512]{1,0:T(8,128)(2,1)} %w_dq.1, bf16[512,512]{1,0:T(8,128)(2,1)} %w_dk.1, ...), custom_call_target="tpu_custom_call" | custom-call | tf_op jit(solution)/shard_map/pallas_call | solution.py:736
  64.5 1.8 %add_convert_fusion = bf16[1,64,2048]{2,1,0:T(8,128)(2,1)} fusion(bf16[2,64,2048]{2,1,0:T(8,128)(2,1)} %shard_map.172), kind=kLoop, calls=%fused_computation | loop fusion | flops 524288 | bytes 786432 | tf_op jit(solution)/shard_map/convert_element_type | solution.py:778
